TPU v7x, 32 devices: a whole 2x2x4 slice. The times are simulated.
32 devices in a mesh: sp: 16 (over z, y, x), tp: 2 (over core).
Axes of the slice: x: 2, y: 2, z: 4, core: 2. Of those that a mesh axis runs over, the one named last changes fastest.
Arguments:
- residual: bfloat16 [3072, 1024], P('sp', 'tp'), may hold values from -6 to 6
- query_first: bfloat16 [3072, 1024], P('sp', 'tp'), may hold values from -64 to 64
- key_first: bfloat16 [3072, 256], P('sp', 'tp'), may hold values from -20 to 20
- value_first: bfloat16 [3072, 256], P('sp', 'tp'), may hold values from -6 to 6
- documents: int32 [3072], P('sp'), may hold values from 0 to 2, as said below
- bias_first: float32 [16, 513], P('tp'), may hold values from -4 to 4
- out_first: bfloat16 [1024, 1024], P('tp'), may hold values from -0.75 to 0.75
- norm_gain: float32 [1024], replicated, may hold values from 0.1 to 1.9
- query_w: bfloat16 [1024, 1024], P(None, 'tp'), may hold values from -0.1875 to 0.1875
- key_w: bfloat16 [1024, 256], P(None, 'tp'), may hold values from -0.1875 to 0.1875
- value_w: bfloat16 [1024, 256], P(None, 'tp'), may hold values from -0.1875 to 0.1875
- bias_second: float32 [16, 513], P('tp'), may hold values from -4 to 4
- out_second: bfloat16 [1024, 1024], P('tp'), may hold values from -0.75 to 0.75
Outputs:
- layer_two: bfloat16 [3072, 1024], P('sp', 'tp')
Inputs may be any that keep to these rules, and one draw needn't show every extreme that they name: Document numbers start at 0, never fall, and rise by one at the first position of each document; there are exactly 3 documents, each of at least 896 positions.
All inputs are finite; a program needn't handle non-finite values.
Results may differ from a plain program's by a relative error of at most 0.017.
Values may be sent and summed in bfloat16 or wider, within the bound.
A program may use at most 64 MiB of HBM per device.

v0:
```python
import functools

import jax
import jax.numpy as jnp
from jax import lax
from jax.experimental import pallas as pl
from jax.experimental.pallas import tpu as pltpu
from jax.sharding import PartitionSpec as P

HEAD_SIZE = 64
SEG = 64
PAST = 4
REL_CLIP = 256
SPAN = PAST * SEG
BAND = SPAN + SEG
LANES = 128
LOG2E = 1.4426950408889634
HIDDEN = -1e30
MESH = pl.DeviceIdType.MESH


eps = 1e-06


def hops_of(tok_rows):
    return range(1, (SPAN + tok_rows - 1) // tok_rows + 1)


def pieces_of(tok_rows):
    pieces = []
    for distance in hops_of(tok_rows):
        top = SPAN - (distance - 1) * tok_rows
        bottom = max(0, top - tok_rows)
        cuts = [cut for cut in range(SEG, tok_rows, SEG) if bottom < cut < top]
        edges = [bottom] + cuts + [top]
        for low, high in reversed(list(zip(edges[:-1], edges[1:]))):
            pieces.append((distance, tok_rows - (top - low), high - low, low))
    return pieces


def build_bias(table_ref, bias_ref):
    heads_local = table_ref.shape[0]
    group_size = bias_ref.shape[2] // SEG
    lane = lax.broadcasted_iota(jnp.int32, (SEG, LANES), 1)
    low = lane < SEG
    last = REL_CLIP + SPAN

    def tile(head, index):
        if index == 0:
            return jnp.broadcast_to(table_ref[head : head + 1, last : last + 1], (SEG, LANES))
        first = last - index * LANES
        return jnp.broadcast_to(table_ref[head : head + 1, first : first + LANES], (SEG, LANES))

    def piece(head, block, base):
        back = block // 2
        if block % 2 == 0:
            source = jnp.where(low, tile(head, back), tile(head, back + 1))
            shift = base
        else:
            source = tile(head, back + 1)
            shift = (base + SEG) % LANES
        return pltpu.roll(source, shift, 1, stride=1, stride_axis=0)

    for head in range(0, heads_local, 2):
        for block in range(PAST + 1):
            pair = jnp.where(low, piece(head, block, 0), piece(head + 1, block, SEG)) * LOG2E
            group, inner = head // group_size, head % group_size
            bias_ref[group, block * SEG : (block + 1) * SEG, inner * SEG : (inner + 2) * SEG] = pair


def attend(segments, query_ref, kv_ref, bias_ref, mask_ref, mixed_ref):
    kv_local = bias_ref.shape[0]
    group_size = bias_ref.shape[2] // SEG
    kv_width = kv_local * HEAD_SIZE
    for segment in segments:
        rows = slice(segment * SEG, (segment + 1) * SEG)
        band = slice(segment * SEG, segment * SEG + BAND)
        mask = mask_ref[segment]
        mask = jnp.concatenate([mask] * (group_size * SEG // LANES), axis=1)
        for group in range(kv_local):
            keys = kv_ref[band, group * HEAD_SIZE : (group + 1) * HEAD_SIZE]
            values = kv_ref[band, kv_width + group * HEAD_SIZE : kv_width + (group + 1) * HEAD_SIZE]
            first = group * group_size
            queries = jnp.concatenate(
                [
                    query_ref[rows, head * HEAD_SIZE : (head + 1) * HEAD_SIZE]
                    for head in range(first, first + group_size)
                ],
                axis=0,
            )
            scores = lax.dot_general(
                keys, queries, (((1,), (1,)), ((), ())), preferred_element_type=jnp.float32
            )
            scores = scores * (HEAD_SIZE ** (-0.5) * LOG2E) + bias_ref[group] + mask
            largest = jnp.max(scores, axis=0, keepdims=True)
            weight = jnp.exp2(scores - largest)
            total = jnp.sum(weight, axis=0, keepdims=True)
            blended = lax.dot_general(
                values,
                weight.astype(jnp.bfloat16),
                (((0,), (0,)), ((), ())),
                preferred_element_type=jnp.float32,
            )
            blended = blended / total
            for pair in range(group_size // 2):
                turned = jnp.transpose(blended[:, pair * LANES : (pair + 1) * LANES])
                both = jnp.concatenate([turned[:SEG], turned[SEG:]], axis=1)
                column = (first + 2 * pair) * HEAD_SIZE
                mixed_ref[rows, column : column + LANES] = both.astype(jnp.bfloat16)


def kernel(
    n_sp,
    key_ref,
    value_ref,
    docs_ref,
    bias_one_ref,
    bias_two_ref,
    gain_ref,
    residual_hbm,
    query_hbm,
    out_one_hbm,
    query_w_hbm,
    key_w_hbm,
    value_w_hbm,
    out_two_hbm,
    result_ref,
    w_out_one,
    w_query,
    w_kv,
    w_out_two,
    kv_one,
    kv_two,
    docs_prior,
    docs_col,
    mask,
    table_one,
    table_two,
    mixed,
    query_one,
    query_two,
    residual_full,
    part_own,
    part_in,
    last_in,
    layer,
    normed,
    send_sem,
    recv_sem,
    load_sem,
):
    me = lax.axis_index("sp")
    my_tp = lax.axis_index("tp")
    other = 1 - my_tp
    tok_rows, width_local = residual_hbm.shape
    kv_width = key_ref.shape[1]
    segments = tok_rows // SEG
    hops = hops_of(tok_rows)
    pieces = pieces_of(tok_rows)
    halves = part_own.shape[0]
    blocks = [(range(segments - 1, 0, -1), SEG, tok_rows - SEG), (range(1), 0, SEG)]

    barrier = pltpu.get_barrier_semaphore()
    expected = jnp.int32(1)
    for distance in hops:
        for step, there in ((distance, me + distance < n_sp), (-distance, me >= distance)):
            expected = expected + there.astype(jnp.int32)

            @pl.when(there)
            def _():
                pl.semaphore_signal(
                    barrier, inc=1, device_id={"sp": me + step}, device_id_type=MESH
                )

    pl.semaphore_signal(barrier, inc=1, device_id={"tp": other}, device_id_type=MESH)

    loads = [
        pltpu.make_async_copy(query_hbm, query_one, load_sem.at[0]),
        pltpu.make_async_copy(out_one_hbm, w_out_one, load_sem.at[1]),
        pltpu.make_async_copy(residual_hbm, residual_full.at[my_tp], load_sem.at[2]),
        pltpu.make_async_copy(key_w_hbm, w_kv.at[:, pl.ds(0, kv_width)], load_sem.at[3]),
        pltpu.make_async_copy(value_w_hbm, w_kv.at[:, pl.ds(kv_width, kv_width)], load_sem.at[4]),
        pltpu.make_async_copy(query_w_hbm, w_query, load_sem.at[5]),
        pltpu.make_async_copy(out_two_hbm, w_out_two, load_sem.at[6]),
    ]
    for load in loads:
        load.start()

    slot = iter(range(send_sem.shape[0]))

    def remote(src, dst, target):
        index = next(slot)
        return pltpu.make_async_remote_copy(
            src_ref=src,
            dst_ref=dst,
            send_sem=send_sem.at[index],
            recv_sem=recv_sem.at[index],
            device_id=target,
            device_id_type=MESH,
        )

    def ahead(distance):
        return {"sp": lax.rem(me + distance, n_sp)}

    def start_sent(distance, copies):
        @pl.when(me + distance < n_sp)
        def _():
            for copy in copies:
                copy.start()

    def wait_arrived(distance, copies):
        @pl.when(me >= distance)
        def _():
            for copy in copies:
                copy.wait_recv()

    def wait_sent(distance, copies):
        @pl.when(me + distance < n_sp)
        def _():
            for copy in copies:
                copy.wait_send()

    pl.semaphore_wait(barrier, expected)

    docs_copies = []
    for distance in hops:
        copies = [remote(docs_ref, docs_prior.at[distance - 1], ahead(distance))]
        docs_copies.append((distance, copies))
        start_sent(distance, copies)
    first_copies = []
    for distance, row, needed, landing in pieces:
        here, there = pl.ds(row, needed), pl.ds(landing, needed)
        copies = [
            remote(key_ref.at[here], kv_one.at[there, pl.ds(0, kv_width)], ahead(distance)),
            remote(value_ref.at[here], kv_one.at[there, pl.ds(kv_width, kv_width)], ahead(distance)),
        ]
        first_copies.append((distance, copies))
        start_sent(distance, copies)
    residual_copy = remote(residual_hbm, residual_full.at[my_tp], {"tp": other})
    residual_copy.start()

    for distance, _, needed, landing in pieces:

        @pl.when(me < distance)
        def _():
            empty = jnp.zeros((needed, 2 * kv_width), jnp.bfloat16)
            kv_one[landing : landing + needed] = empty
            kv_two[landing : landing + needed] = empty

    for distance in hops:

        @pl.when(me < distance)
        def _():
            docs_prior[distance - 1] = jnp.full((1, tok_rows), -1, jnp.int32)

    kv_one[SPAN:, :kv_width] = key_ref[...]
    kv_one[SPAN:, kv_width:] = value_ref[...]

    build_bias(bias_one_ref, table_one)
    build_bias(bias_two_ref, table_two)

    for distance, copies in docs_copies:
        wait_arrived(distance, copies)

    eye = lax.broadcasted_iota(jnp.int32, (SEG, SEG), 0) == lax.broadcasted_iota(
        jnp.int32, (SEG, SEG), 1
    )

    def put_column(docs, place):
        picked = jnp.where(eye, docs.astype(jnp.float32), 0.0)
        docs_col[place : place + SEG] = jnp.broadcast_to(
            jnp.sum(picked, axis=1, keepdims=True), (SEG, LANES)
        )

    for distance, row, needed, landing in pieces:
        for block in range(0, needed, SEG):
            put_column(
                docs_prior[distance - 1, :, row + block : row + block + SEG], landing + block
            )
    for block in range(0, tok_rows, SEG):
        put_column(docs_ref[:, block : block + SEG], SPAN + block)
    for segment in range(segments):
        own = docs_ref[:, segment * SEG : (segment + 1) * SEG].astype(jnp.float32)
        own = jnp.concatenate([own, own], axis=1)
        same = docs_col[segment * SEG : segment * SEG + BAND] == own
        mask[segment] = jnp.where(same, 0.0, HIDDEN)

    def attend_block(members, waiting, *refs):
        for segment in members:
            for (distance, _, needed, landing), (_, copies) in zip(pieces, waiting):
                reached = landing + needed > segment * SEG
                earlier = landing + needed > (segment + 1) * SEG
                if reached and not (earlier and segment + 1 < segments):
                    wait_arrived(distance, copies)
            attend([segment], *refs)

    loads[0].wait()
    part_copies = []
    for members, start, count in blocks:
        attend_block(members, first_copies, query_one, kv_one, table_one, mask, mixed)
        if start > 0:
            loads[1].wait()
        rows = pl.ds(start, count)
        copies = []
        for half in range(halves):
            part_own[half, start : start + count] = jnp.dot(
                mixed[start : start + count],
                w_out_one[:, half * width_local : (half + 1) * width_local],
                preferred_element_type=jnp.float32,
            ).astype(jnp.bfloat16)
            copy = remote(part_own.at[half, rows], part_in.at[half, rows], {"tp": other})
            copy.start()
            copies.append(copy)
        part_copies.append(copies)

    loads[2].wait()
    residual_copy.wait_recv()
    second_copies = [None] * len(pieces)
    for (_, start, count), copies in zip(blocks, part_copies):
        rows = slice(start, start + count)
        squares = jnp.zeros((count, 1), jnp.float32)
        for half in range(halves):
            copies[half].wait_recv()
            new = residual_full[half, rows].astype(jnp.float32) + (
                part_own[half, rows].astype(jnp.float32) + part_in[half, rows].astype(jnp.float32)
            )
            new = new.astype(jnp.bfloat16)
            layer[half, rows] = new
            new = new.astype(jnp.float32)
            squares = squares + jnp.sum(new * new, axis=1, keepdims=True)
        scale = lax.rsqrt(squares / (halves * width_local) + eps)
        for half in range(halves):
            columns = slice(half * width_local, (half + 1) * width_local)
            normed[rows, columns] = (
                layer[half, rows].astype(jnp.float32) * scale * gain_ref[:, columns]
            ).astype(jnp.bfloat16)
        if start > 0:
            loads[3].wait()
            loads[4].wait()
        kv_two[SPAN + start : SPAN + start + count] = jnp.dot(
            normed[rows], w_kv[...], preferred_element_type=jnp.float32
        ).astype(jnp.bfloat16)
        for index, (distance, row, needed, landing) in enumerate(pieces):
            if start <= row < start + count:
                piece = remote(
                    kv_two.at[pl.ds(SPAN + row, needed)],
                    kv_two.at[pl.ds(landing, needed)],
                    ahead(distance),
                )
                second_copies[index] = (distance, [piece])
                start_sent(distance, [piece])
    loads[5].wait()
    query_two[...] = jnp.dot(normed[...], w_query[...], preferred_element_type=jnp.float32).astype(
        jnp.bfloat16
    )
    for copies in part_copies:
        for copy in copies:
            copy.wait_send()

    loads[6].wait()
    theirs = pl.ds(pl.multiple_of(other * width_local, width_local), width_local)
    ours = pl.ds(pl.multiple_of(my_tp * width_local, width_local), width_local)
    last_copies = []
    for members, start, count in blocks:
        attend_block(members, second_copies, query_two, kv_two, table_two, mask, mixed)
        rows = pl.ds(start, count)
        part_own[0, start : start + count] = jnp.dot(
            mixed[start : start + count], w_out_two[:, theirs], preferred_element_type=jnp.float32
        ).astype(jnp.bfloat16)
        copy = remote(part_own.at[0, rows], last_in.at[rows], {"tp": other})
        copy.start()
        last_copies.append(copy)
    part_own[1] = jnp.dot(
        mixed[...], w_out_two[:, ours], preferred_element_type=jnp.float32
    ).astype(jnp.bfloat16)
    for (_, start, count), copy in zip(blocks, last_copies):
        rows = slice(start, start + count)
        copy.wait_recv()
        branch = part_own[1, rows].astype(jnp.float32) + last_in[rows].astype(jnp.float32)
        result_ref[rows] = (layer[my_tp, rows].astype(jnp.float32) + branch).astype(jnp.bfloat16)

    residual_copy.wait_send()
    for distance, copies in docs_copies + first_copies + second_copies:
        wait_sent(distance, copies)
    for copy in last_copies:
        copy.wait_send()


def body(
    residual,
    query_first,
    key_first,
    value_first,
    documents,
    bias_first,
    out_first,
    norm_gain,
    query_w,
    key_w,
    value_w,
    bias_second,
    out_second,
):
    n_sp = lax.axis_size("sp")
    tok_rows, width_local = residual.shape
    query_width = query_first.shape[1]
    kv_width = key_first.shape[1]
    kv_local = kv_width // HEAD_SIZE
    group_width = query_width // kv_local
    halves = out_first.shape[1] // width_local
    hops = len(hops_of(tok_rows))
    n_sems = hops + 3 * len(pieces_of(tok_rows)) + 1 + 2 * halves + 2
    vmem = pl.BlockSpec(memory_space=pltpu.VMEM)
    hbm = pl.BlockSpec(memory_space=pl.ANY)
    bf16 = jnp.bfloat16
    return pl.pallas_call(
        functools.partial(kernel, n_sp),
        name="two_layers",
        out_shape=pltpu.VMEM((tok_rows, width_local), bf16),
        in_specs=[vmem] * 6 + [hbm] * 7,
        out_specs=vmem,
        scratch_shapes=[
            pltpu.VMEM(out_first.shape, bf16),
            pltpu.VMEM(query_w.shape, bf16),
            pltpu.VMEM((key_w.shape[0], 2 * kv_width), bf16),
            pltpu.VMEM(out_second.shape, bf16),
            pltpu.VMEM((SPAN + tok_rows, 2 * kv_width), bf16),
            pltpu.VMEM((SPAN + tok_rows, 2 * kv_width), bf16),
            pltpu.VMEM((hops, 1, tok_rows), jnp.int32),
            pltpu.VMEM((SPAN + tok_rows, LANES), jnp.float32),
            pltpu.VMEM((tok_rows // SEG, BAND, LANES), jnp.float32),
            pltpu.VMEM((kv_local, BAND, group_width), jnp.float32),
            pltpu.VMEM((kv_local, BAND, group_width), jnp.float32),
            pltpu.VMEM((tok_rows, query_width), bf16),
            pltpu.VMEM((tok_rows, query_width), bf16),
            pltpu.VMEM((tok_rows, query_width), bf16),
            pltpu.VMEM((halves, tok_rows, width_local), bf16),
            pltpu.VMEM((halves, tok_rows, width_local), bf16),
            pltpu.VMEM((halves, tok_rows, width_local), bf16),
            pltpu.VMEM((tok_rows, width_local), bf16),
            pltpu.VMEM((halves, tok_rows, width_local), bf16),
            pltpu.VMEM((tok_rows, halves * width_local), bf16),
            pltpu.SemaphoreType.DMA((n_sems,)),
            pltpu.SemaphoreType.DMA((n_sems,)),
            pltpu.SemaphoreType.DMA((7,)),
        ],
        compiler_params=pltpu.CompilerParams(collective_id=0, has_side_effects=True),
    )(
        key_first,
        value_first,
        documents.reshape(1, tok_rows),
        bias_first,
        bias_second,
        norm_gain.reshape(1, -1),
        residual,
        query_first,
        out_first,
        query_w,
        key_w,
        value_w,
        out_second,
    )


def solution(mesh):
    placed = (
        P("sp", "tp"),
        P("sp", "tp"),
        P("sp", "tp"),
        P("sp", "tp"),
        P("sp"),
        P("tp", None),
        P("tp", None),
        P(),
        P(None, "tp"),
        P(None, "tp"),
        P(None, "tp"),
        P("tp", None),
        P("tp", None),
    )
    return jax.shard_map(body, mesh=mesh, in_specs=placed, out_specs=P("sp", "tp"), check_vma=False)
```

profile of v0, /device:TPU:25, one launch (start us, length us, event | category | flops | bytes accessed | tf_op | source)
XLA Modules:
  0.0 20.9 jit_solution(14482670849832382924)
XLA Ops:
  0.0 20.2 %two_layers.1 = bf16[192,512]{1,0:T(8,128)(2,1)S(1)} custom-call(bf16[192,128]{1,0:T(8,128)(2,1)} %key_ref.1, bf16[192,128]{1,0:T(8,128)(2,1)} %value_ref.1, s32[1,192]{1,0:T(1,128)} %bitcast.3, f32[8,513]{1,0:T(8,128)} %bias_one_ref.1, f32[8,513]{1,0:T(8,128)} %bias_two_ref.1, f32[1,1024]{1,0:T(1,128)} %bitcast.2, bf16[192,512]{1,0:T(8,128)(2,1)} %residual_hbm.1, ...), custom_call_target="tpu_custom_call" | custom-call | tf_op jit(solution)/shard_map/two_layers/pallas_call | solution.py:416
  20.2 0.7 %copy.15 = bf16[192,512]{1,0:T(8,128)(2,1)} copy(bf16[192,512]{1,0:T(8,128)(2,1)S(1)} %two_layers.1) | data formatting | bytes 393216
where the time goes:
time: 21.1 us; the launch traced here: 20.9 us
  Pallas kernels  20.2 us (96%)
  local copies, waits for them, and re-layouts  0.68 us (3%)
    pallas_call x1, Pallas kernels, body(): pl.pallas_call(functools.partial(kernel, n_sp), name='two_layers', out_sh...  20.2 us
    unnamed x1, local copies, waits for them, and re-layouts  0.68 us

commit v1 on v0

v1 whole, which is shorter than its diff:
```python
import functools

import jax
import jax.numpy as jnp
from jax import lax
from jax.experimental import pallas as pl
from jax.experimental.pallas import tpu as pltpu
from jax.sharding import PartitionSpec as P

HEAD_SIZE = 64
SEG = 64
PAST = 4
REL_CLIP = 256
SPAN = PAST * SEG
BAND = SPAN + SEG
LANES = 128
LOG2E = 1.4426950408889634
HIDDEN = -1e30
MESH = pl.DeviceIdType.MESH


eps = 1e-06


def hops_of(tok_rows):
    return range(1, (SPAN + tok_rows - 1) // tok_rows + 1)


def pieces_of(tok_rows):
    pieces = []
    for distance in hops_of(tok_rows):
        top = SPAN - (distance - 1) * tok_rows
        bottom = max(0, top - tok_rows)
        cuts = [cut for cut in range(SEG, tok_rows, SEG) if bottom < cut < top]
        edges = [bottom] + cuts + [top]
        for low, high in reversed(list(zip(edges[:-1], edges[1:]))):
            pieces.append((distance, tok_rows - (top - low), high - low, low))
    return pieces


def build_bias(table_ref, bias_ref):
    heads_local = table_ref.shape[0]
    group_size = bias_ref.shape[2] // SEG
    lane = lax.broadcasted_iota(jnp.int32, (SEG, LANES), 1)
    low = lane < SEG
    last = REL_CLIP + SPAN

    def tile(head, index):
        if index == 0:
            return jnp.broadcast_to(table_ref[head : head + 1, last : last + 1], (SEG, LANES))
        first = last - index * LANES
        return jnp.broadcast_to(table_ref[head : head + 1, first : first + LANES], (SEG, LANES))

    def piece(head, block, base):
        back = block // 2
        if block % 2 == 0:
            source = jnp.where(low, tile(head, back), tile(head, back + 1))
            shift = base
        else:
            source = tile(head, back + 1)
            shift = (base + SEG) % LANES
        return pltpu.roll(source, shift, 1, stride=1, stride_axis=0)

    for head in range(0, heads_local, 2):
        for block in range(PAST + 1):
            pair = jnp.where(low, piece(head, block, 0), piece(head + 1, block, SEG)) * LOG2E
            group, inner = head // group_size, head % group_size
            bias_ref[group, block * SEG : (block + 1) * SEG, inner * SEG : (inner + 2) * SEG] = pair


class Attention:
    def __init__(self, query, kv, bias, mask, mixed, padded, turned, scores, weights, stats, blend):
        self.query, self.kv, self.bias, self.mask, self.mixed = query, kv, bias, mask, mixed
        self.padded, self.turned, self.scores, self.weights = padded, turned, scores, weights
        self.stats, self.blend = stats, blend
        self.groups = bias.shape[0]
        self.group_size = bias.shape[2] // SEG
        self.kv_width = self.groups * HEAD_SIZE
        self.state = {}

    def unit(self, segment, group):
        return segment * self.groups + group

    def pad_queries(self, segment):
        lane = lax.broadcasted_iota(jnp.int32, (SEG, LANES), 1)
        rows = slice(segment * SEG, (segment + 1) * SEG)
        for group in range(self.groups):
            keep = (lane >= group * HEAD_SIZE) & (lane < (group + 1) * HEAD_SIZE)
            for inner in range(self.group_size):
                head = group * self.group_size + inner
                column = head * HEAD_SIZE // LANES * LANES
                block = self.query[rows, column : column + LANES]
                if head % 2 != group % 2:
                    block = jnp.concatenate([block[:, HEAD_SIZE:], block[:, :HEAD_SIZE]], axis=1)
                self.padded[self.unit(segment, group), inner * SEG : (inner + 1) * SEG] = jnp.where(
                    keep, block, jnp.zeros_like(block)
                )

    def turn_values(self, row):
        block = jnp.transpose(self.kv[row : row + SEG, self.kv_width : 2 * self.kv_width])
        self.turned[0, :, row : row + SEG] = block
        if row >= SEG:
            self.turned[1, :, row - SEG : row] = block

    def bounds(self, segment, local):
        first = segment * SEG
        return (max(first, SPAN), first + BAND) if local else (first, SPAN)

    def score(self, segment, group, local):
        low, high = self.bounds(segment, local)
        unit = self.unit(segment, group)
        band = slice(low - segment * SEG, high - segment * SEG)
        scores = lax.dot_general(
            self.kv[low:high, : self.kv_width],
            self.padded[unit],
            (((1,), (1,)), ((), ())),
            preferred_element_type=jnp.float32,
        )
        mask = self.mask[segment, band]
        mask = jnp.concatenate([mask] * (self.group_size * SEG // LANES), axis=1)
        scores = scores * (HEAD_SIZE ** (-0.5) * LOG2E) + self.bias[group, band] + mask
        self.scores[unit, band] = scores
        largest = jnp.max(scores, axis=0, keepdims=True)
        if local:
            self.stats[unit, 0:1] = largest
        else:
            largest = jnp.maximum(largest, self.stats[unit, 0:1])
        self.state[unit] = (largest,)

    def weigh(self, segment, group, local):
        low, high = self.bounds(segment, local)
        unit = self.unit(segment, group)
        band = slice(low - segment * SEG, high - segment * SEG)
        (largest,) = self.state[unit]
        weight = jnp.exp2(self.scores[unit, band] - largest)
        self.weights[unit, band] = weight.astype(jnp.bfloat16)
        total = jnp.sum(weight, axis=0, keepdims=True)
        if local:
            self.stats[unit, 1:2] = total
        else:
            fade = jnp.exp2(self.stats[unit, 0:1] - largest)
            inverse = 1.0 / (total + self.stats[unit, 1:2] * fade)
            self.state[unit] = (fade, inverse)

    def gather(self, segment, group, local):
        low, high = self.bounds(segment, local)
        unit = self.unit(segment, group)
        band = slice(low - segment * SEG, high - segment * SEG)
        odd = low // SEG % 2
        blended = lax.dot_general(
            self.turned[
                odd,
                group * HEAD_SIZE : (group + 1) * HEAD_SIZE,
                low - odd * SEG : high - odd * SEG,
            ],
            self.weights[unit, band],
            (((1,), (0,)), ((), ())),
            preferred_element_type=jnp.float32,
        )
        if local:
            self.blend[unit] = blended
            return
        fade, inverse = self.state[unit]
        blended = (blended + self.blend[unit] * fade) * inverse
        rows = slice(segment * SEG, (segment + 1) * SEG)
        for pair in range(self.group_size // 2):
            turned = jnp.transpose(blended[:, pair * LANES : (pair + 1) * LANES])
            both = jnp.concatenate([turned[:SEG], turned[SEG:]], axis=1)
            column = (group * self.group_size + 2 * pair) * HEAD_SIZE
            self.mixed[rows, column : column + LANES] = both.astype(jnp.bfloat16)

    def run(self, segments, local):
        units = [(segment, group) for segment in segments for group in range(self.groups)]
        self.score(*units[0], local)
        for index in range(len(units)):
            if index + 1 < len(units):
                self.score(*units[index + 1], local)
            if index > 0:
                self.gather(*units[index - 1], local)
            self.weigh(*units[index], local)
        self.gather(*units[-1], local)


def kernel(
    n_sp,
    residual_hbm,
    query_hbm,
    key_hbm,
    value_hbm,
    docs_hbm,
    bias_one_hbm,
    out_one_hbm,
    gain_hbm,
    query_w_hbm,
    key_w_hbm,
    value_w_hbm,
    bias_two_hbm,
    out_two_hbm,
    result_ref,
    w_out_one,
    w_query,
    w_kv,
    w_out_two,
    bias_one,
    bias_two,
    gain,
    docs,
    kv_one,
    kv_two,
    docs_prior,
    docs_col,
    mask,
    table_one,
    table_two,
    mixed,
    query_one,
    query_two,
    residual_full,
    part_own,
    part_in,
    last_in,
    layer,
    normed,
    padded,
    turned,
    scores,
    weights,
    stats,
    blend,
    send_sem,
    recv_sem,
    load_sem,
):
    me = lax.axis_index("sp")
    my_tp = lax.axis_index("tp")
    other = 1 - my_tp
    tok_rows, width_local = residual_hbm.shape
    kv_width = key_hbm.shape[1]
    segments = tok_rows // SEG
    hops = hops_of(tok_rows)
    pieces = pieces_of(tok_rows)
    halves = part_own.shape[0]
    blocks = [(range(segments - 1, 0, -1), SEG, tok_rows - SEG), (range(1), 0, SEG)]

    barrier = pltpu.get_barrier_semaphore()
    expected = jnp.int32(1)
    for distance in hops:
        expected = expected + (me + distance < n_sp).astype(jnp.int32)

        @pl.when(me >= distance)
        def _():
            pl.semaphore_signal(
                barrier, inc=1, device_id={"sp": me - distance}, device_id_type=MESH
            )

    pl.semaphore_signal(barrier, inc=1, device_id={"tp": other}, device_id_type=MESH)

    own = pl.ds(SPAN, tok_rows)
    transfers = dict(
        bias_one=(bias_one_hbm, bias_one),
        key=(key_hbm, kv_one.at[own, pl.ds(0, kv_width)]),
        value=(value_hbm, kv_one.at[own, pl.ds(kv_width, kv_width)]),
        docs=(docs_hbm, docs),
        query=(query_hbm, query_one),
        residual=(residual_hbm, residual_full.at[my_tp]),
        bias_two=(bias_two_hbm, bias_two),
        out_one=(out_one_hbm, w_out_one),
        gain=(gain_hbm, gain),
        key_w=(key_w_hbm, w_kv.at[:, pl.ds(0, kv_width)]),
        value_w=(value_w_hbm, w_kv.at[:, pl.ds(kv_width, kv_width)]),
        query_w=(query_w_hbm, w_query),
        out_two=(out_two_hbm, w_out_two),
    )
    loads = {
        name: pltpu.make_async_copy(src, dst, load_sem.at[index])
        for index, (name, (src, dst)) in enumerate(transfers.items())
    }
    for load in loads.values():
        load.start()

    slot = iter(range(send_sem.shape[0]))

    def remote(src, dst, target):
        index = next(slot)
        return pltpu.make_async_remote_copy(
            src_ref=src,
            dst_ref=dst,
            send_sem=send_sem.at[index],
            recv_sem=recv_sem.at[index],
            device_id=target,
            device_id_type=MESH,
        )

    def ahead(distance):
        return {"sp": lax.rem(me + distance, n_sp)}

    def start_sent(distance, copies):
        @pl.when(me + distance < n_sp)
        def _():
            for copy in copies:
                copy.start()

    def wait_arrived(distance, copies):
        @pl.when(me >= distance)
        def _():
            for copy in copies:
                copy.wait_recv()

    def wait_sent(distance, copies):
        @pl.when(me + distance < n_sp)
        def _():
            for copy in copies:
                copy.wait_send()

    for distance, _, needed, landing in pieces:

        @pl.when(me < distance)
        def _():
            empty = jnp.zeros((needed, 2 * kv_width), jnp.bfloat16)
            kv_one[landing : landing + needed] = empty
            kv_two[landing : landing + needed] = empty

    for distance in hops:

        @pl.when(me < distance)
        def _():
            docs_prior[distance - 1] = jnp.full((1, tok_rows), -1, jnp.int32)

    loads["bias_one"].wait()
    build_bias(bias_one, table_one)
    for name in ("key", "value", "docs"):
        loads[name].wait()

    pl.semaphore_wait(barrier, expected)

    def halo_copy(kv, piece):
        distance, row, needed, landing = piece
        return remote(
            kv.at[pl.ds(SPAN + row, needed)], kv.at[pl.ds(landing, needed)], ahead(distance)
        )

    docs_copies = [
        (distance, [remote(docs, docs_prior.at[distance - 1], ahead(distance))])
        for distance in hops
    ]
    first_copies = [(piece[0], [halo_copy(kv_one, piece)]) for piece in pieces]
    for distance, copies in docs_copies + first_copies:
        start_sent(distance, copies)
    loads["residual"].wait()
    residual_copy = remote(
        residual_full.at[my_tp], residual_full.at[my_tp], {"tp": other}
    )
    residual_copy.start()

    eye = lax.broadcasted_iota(jnp.int32, (SEG, SEG), 0) == lax.broadcasted_iota(
        jnp.int32, (SEG, SEG), 1
    )

    def put_column(numbers, place):
        picked = jnp.where(eye, numbers.astype(jnp.float32), 0.0)
        docs_col[place : place + SEG] = jnp.broadcast_to(
            jnp.sum(picked, axis=1, keepdims=True), (SEG, LANES)
        )

    def put_mask(segment, low, high):
        mine = docs[:, segment * SEG : (segment + 1) * SEG].astype(jnp.float32)
        mine = jnp.concatenate([mine, mine], axis=1)
        same = docs_col[low:high] == mine
        first = segment * SEG
        mask[segment, low - first : high - first] = jnp.where(same, 0.0, HIDDEN)

    shared = (mask, mixed, padded, turned, scores, weights, stats, blend)
    one = Attention(query_one, kv_one, table_one, *shared)
    two = Attention(query_two, kv_two, table_two, *shared)
    newest_first = range(segments - 1, -1, -1)

    for block in range(0, tok_rows, SEG):
        put_column(docs[:, block : block + SEG], SPAN + block)
    for segment in range(segments):
        put_mask(segment, *one.bounds(segment, True))

    loads["query"].wait()
    for row in range(SPAN, SPAN + tok_rows, SEG):
        one.turn_values(row)
    for segment in newest_first:
        one.pad_queries(segment)
    one.run(newest_first, True)

    loads["bias_two"].wait()
    build_bias(bias_two, table_two)

    for distance, copies in docs_copies:
        wait_arrived(distance, copies)
    for distance, row, needed, landing in pieces:
        for block in range(0, needed, SEG):
            put_column(
                docs_prior[distance - 1, :, row + block : row + block + SEG], landing + block
            )
    for segment in range(segments):
        put_mask(segment, *one.bounds(segment, False))

    def halo_block(layer_attention, members, waiting, done):
        for piece, (distance, copies) in zip(pieces, waiting):
            _, _, needed, landing = piece
            if landing + needed > min(members) * SEG and landing not in done:
                done.add(landing)
                wait_arrived(distance, copies)
                for row in range(landing, landing + needed, SEG):
                    layer_attention.turn_values(row)
        layer_attention.run(members, False)

    part_copies = []
    done = set()
    for members, start, count in blocks:
        halo_block(one, members, first_copies, done)
        if start > 0:
            loads["out_one"].wait()
        rows = pl.ds(start, count)
        copies = []
        for half in range(halves):
            part_own[half, start : start + count] = jnp.dot(
                mixed[start : start + count],
                w_out_one[:, half * width_local : (half + 1) * width_local],
                preferred_element_type=jnp.float32,
            ).astype(jnp.bfloat16)
            copy = remote(part_own.at[half, rows], part_in.at[half, rows], {"tp": other})
            copy.start()
            copies.append(copy)
        part_copies.append(copies)

    residual_copy.wait_recv()
    second_copies = [None] * len(pieces)
    for (_, start, count), copies in zip(blocks, part_copies):
        rows = slice(start, start + count)
        squares = jnp.zeros((count, 1), jnp.float32)
        for half in range(halves):
            copies[half].wait_recv()
            new = residual_full[half, rows].astype(jnp.float32) + (
                part_own[half, rows].astype(jnp.float32) + part_in[half, rows].astype(jnp.float32)
            )
            new = new.astype(jnp.bfloat16)
            layer[half, rows] = new
            new = new.astype(jnp.float32)
            squares = squares + jnp.sum(new * new, axis=1, keepdims=True)
        if start > 0:
            loads["gain"].wait()
        scale = lax.rsqrt(squares / (halves * width_local) + eps)
        for half in range(halves):
            columns = slice(half * width_local, (half + 1) * width_local)
            normed[rows, columns] = (
                layer[half, rows].astype(jnp.float32) * scale * gain[:, columns]
            ).astype(jnp.bfloat16)
        if start > 0:
            loads["key_w"].wait()
            loads["value_w"].wait()
        kv_two[SPAN + start : SPAN + start + count] = jnp.dot(
            normed[rows], w_kv[...], preferred_element_type=jnp.float32
        ).astype(jnp.bfloat16)
        for index, piece in enumerate(pieces):
            if start <= piece[1] < start + count:
                second_copies[index] = (piece[0], [halo_copy(kv_two, piece)])
                start_sent(*second_copies[index])
    loads["query_w"].wait()
    query_two[...] = jnp.dot(normed[...], w_query[...], preferred_element_type=jnp.float32).astype(
        jnp.bfloat16
    )
    for row in range(SPAN, SPAN + tok_rows, SEG):
        two.turn_values(row)
    for segment in newest_first:
        two.pad_queries(segment)
    two.run(newest_first, True)
    for copies in part_copies:
        for copy in copies:
            copy.wait_send()

    loads["out_two"].wait()
    theirs = pl.ds(pl.multiple_of(other * width_local, width_local), width_local)
    ours = pl.ds(pl.multiple_of(my_tp * width_local, width_local), width_local)
    last_copies = []
    done = set()
    for members, start, count in blocks:
        halo_block(two, members, second_copies, done)
        rows = pl.ds(start, count)
        part_own[0, start : start + count] = jnp.dot(
            mixed[start : start + count], w_out_two[:, theirs], preferred_element_type=jnp.float32
        ).astype(jnp.bfloat16)
        copy = remote(part_own.at[0, rows], last_in.at[rows], {"tp": other})
        copy.start()
        last_copies.append(copy)
    part_own[1] = jnp.dot(
        mixed[...], w_out_two[:, ours], preferred_element_type=jnp.float32
    ).astype(jnp.bfloat16)
    for (_, start, count), copy in zip(blocks, last_copies):
        rows = slice(start, start + count)
        copy.wait_recv()
        branch = part_own[1, rows].astype(jnp.float32) + last_in[rows].astype(jnp.float32)
        result_ref[rows] = (layer[my_tp, rows].astype(jnp.float32) + branch).astype(jnp.bfloat16)

    residual_copy.wait_send()
    for distance, copies in docs_copies + first_copies + second_copies:
        wait_sent(distance, copies)
    for copy in last_copies:
        copy.wait_send()


def body(
    residual,
    query_first,
    key_first,
    value_first,
    documents,
    bias_first,
    out_first,
    norm_gain,
    query_w,
    key_w,
    value_w,
    bias_second,
    out_second,
):
    n_sp = lax.axis_size("sp")
    tok_rows, width_local = residual.shape
    query_width = query_first.shape[1]
    kv_width = key_first.shape[1]
    kv_local = kv_width // HEAD_SIZE
    group_width = query_width // kv_local
    halves = out_first.shape[1] // width_local
    hops = len(hops_of(tok_rows))
    units = tok_rows // SEG * kv_local
    n_sems = hops + 2 * len(pieces_of(tok_rows)) + 1 + 2 * halves + 2
    vmem = pl.BlockSpec(memory_space=pltpu.VMEM)
    hbm = pl.BlockSpec(memory_space=pl.ANY)
    bf16 = jnp.bfloat16
    f32 = jnp.float32
    return pl.pallas_call(
        functools.partial(kernel, n_sp),
        name="two_layers",
        out_shape=pltpu.VMEM((tok_rows, width_local), bf16),
        in_specs=[hbm] * 13,
        out_specs=vmem,
        scratch_shapes=[
            pltpu.VMEM(out_first.shape, bf16),
            pltpu.VMEM(query_w.shape, bf16),
            pltpu.VMEM((key_w.shape[0], 2 * kv_width), bf16),
            pltpu.VMEM(out_second.shape, bf16),
            pltpu.VMEM(bias_first.shape, f32),
            pltpu.VMEM(bias_second.shape, f32),
            pltpu.VMEM((1, norm_gain.shape[0]), f32),
            pltpu.VMEM((1, tok_rows), jnp.int32),
            pltpu.VMEM((SPAN + tok_rows, 2 * kv_width), bf16),
            pltpu.VMEM((SPAN + tok_rows, 2 * kv_width), bf16),
            pltpu.VMEM((hops, 1, tok_rows), jnp.int32),
            pltpu.VMEM((SPAN + tok_rows, LANES), f32),
            pltpu.VMEM((tok_rows // SEG, BAND, LANES), f32),
            pltpu.VMEM((kv_local, BAND, group_width), f32),
            pltpu.VMEM((kv_local, BAND, group_width), f32),
            pltpu.VMEM((tok_rows, query_width), bf16),
            pltpu.VMEM((tok_rows, query_width), bf16),
            pltpu.VMEM((tok_rows, query_width), bf16),
            pltpu.VMEM((halves, tok_rows, width_local), bf16),
            pltpu.VMEM((halves, tok_rows, width_local), bf16),
            pltpu.VMEM((halves, tok_rows, width_local), bf16),
            pltpu.VMEM((tok_rows, width_local), bf16),
            pltpu.VMEM((halves, tok_rows, width_local), bf16),
            pltpu.VMEM((tok_rows, halves * width_local), bf16),
            pltpu.VMEM((units, group_width, LANES), bf16),
            pltpu.VMEM((2, kv_width, pl.cdiv(SPAN + tok_rows, LANES) * LANES), bf16),
            pltpu.VMEM((units, BAND, group_width), f32),
            pltpu.VMEM((units, BAND, group_width), bf16),
            pltpu.VMEM((units, 2, group_width), f32),
            pltpu.VMEM((units, HEAD_SIZE, group_width), f32),
            pltpu.SemaphoreType.DMA((n_sems,)),
            pltpu.SemaphoreType.DMA((n_sems,)),
            pltpu.SemaphoreType.DMA((13,)),
        ],
        compiler_params=pltpu.CompilerParams(collective_id=0, has_side_effects=True),
    )(
        residual,
        query_first,
        key_first,
        value_first,
        documents.reshape(1, tok_rows),
        bias_first,
        out_first,
        norm_gain.reshape(1, -1),
        query_w,
        key_w,
        value_w,
        bias_second,
        out_second,
    )


def solution(mesh):
    placed = (
        P("sp", "tp"),
        P("sp", "tp"),
        P("sp", "tp"),
        P("sp", "tp"),
        P("sp"),
        P("tp", None),
        P("tp", None),
        P(),
        P(None, "tp"),
        P(None, "tp"),
        P(None, "tp"),
        P("tp", None),
        P("tp", None),
    )
    return jax.shard_map(body, mesh=mesh, in_specs=placed, out_specs=P("sp", "tp"), check_vma=False)
```

time: 21.1 us -> 18.7 us (0.89)
  Pallas kernels: 20.2 us -> 17.8 us
    pallas_call x1, Pallas kernels: 20.2 us -> 17.8 us  [body(): pl.pallas_call(functools.partial(kernel, n_sp), name='two_layers', out_sh...]
where the time goes in v1:
time: 18.7 us; the launch traced here: 18.5 us
  Pallas kernels  17.8 us (95%)
  local copies, waits for them, and re-layouts  0.68 us (4%)
    pallas_call x1, Pallas kernels, body(): pl.pallas_call(functools.partial(kernel, n_sp), name='two_layers', out_sh...  17.8 us
    unnamed x1, local copies, waits for them, and re-layouts  0.68 us

profile of v1, /device:TPU:25, one launch (start us, length us, event | category | flops | bytes accessed | tf_op | source)
XLA Modules:
  0.0 18.5 jit_solution(2949468631768953845)
XLA Ops:
  0.0 17.8 %two_layers.1 = bf16[192,512]{1,0:T(8,128)(2,1)S(1)} custom-call(bf16[192,512]{1,0:T(8,128)(2,1)} %residual_hbm.1, bf16[192,512]{1,0:T(8,128)(2,1)} %query_hbm.1, bf16[192,128]{1,0:T(8,128)(2,1)} %key_hbm.1, bf16[192,128]{1,0:T(8,128)(2,1)} %value_hbm.1, s32[1,192]{1,0:T(1,128)} %bitcast.3, f32[8,513]{1,0:T(8,128)} %bias_one_hbm.1, ...), custom_call_target="tpu_custom_call" | custom-call | tf_op jit(solution)/shard_map/two_layers/pallas_call | solution.py:535
  17.8 0.7 %copy.15 = bf16[192,512]{1,0:T(8,128)(2,1)} copy(bf16[192,512]{1,0:T(8,128)(2,1)S(1)} %two_layers.1) | data formatting | bytes 393216

commit v2 on v1

--- a/solution.py
+++ b/solution.py
@@ -169,16 +169,27 @@
             column = (group * self.group_size + 2 * pair) * HEAD_SIZE
             self.mixed[rows, column : column + LANES] = both.astype(jnp.bfloat16)
 
-    def run(self, segments, local):
+    def run(self, segments, local, before=None, after=None):
         units = [(segment, group) for segment in segments for group in range(self.groups)]
-        self.score(*units[0], local)
-        for index in range(len(units)):
+
+        def score(unit):
+            if before is not None:
+                before(unit[0])
+            self.score(*unit, local)
+
+        def gather(unit):
+            self.gather(*unit, local)
+            if after is not None and unit[1] == self.groups - 1:
+                after(unit[0])
+
+        score(units[0])
+        for index, unit in enumerate(units):
             if index + 1 < len(units):
-                self.score(*units[index + 1], local)
+                score(units[index + 1])
             if index > 0:
-                self.gather(*units[index - 1], local)
-            self.weigh(*units[index], local)
-        self.gather(*units[-1], local)
+                gather(units[index - 1])
+            self.weigh(*unit, local)
+        gather(units[-1])
 
 
 def kernel(
@@ -220,7 +231,9 @@
     part_in,
     last_in,
     layer,
-    normed,
+    base,
+    scaled,
+    scales,
     padded,
     turned,
     scores,
@@ -326,10 +339,38 @@
         def _():
             docs_prior[distance - 1] = jnp.full((1, tok_rows), -1, jnp.int32)
 
-    loads["bias_one"].wait()
-    build_bias(bias_one, table_one)
-    for name in ("key", "value", "docs"):
+    eye = lax.broadcasted_iota(jnp.int32, (SEG, SEG), 0) == lax.broadcasted_iota(
+        jnp.int32, (SEG, SEG), 1
+    )
+
+    def put_column(numbers, place):
+        picked = jnp.where(eye, numbers.astype(jnp.float32), 0.0)
+        docs_col[place : place + SEG] = jnp.broadcast_to(
+            jnp.sum(picked, axis=1, keepdims=True), (SEG, LANES)
+        )
+
+    def put_mask(segment, low, high):
+        mine = docs[:, segment * SEG : (segment + 1) * SEG].astype(jnp.float32)
+        mine = jnp.concatenate([mine, mine], axis=1)
+        same = docs_col[low:high] == mine
+        first = segment * SEG
+        mask[segment, low - first : high - first] = jnp.where(same, 0.0, HIDDEN)
+
+    shared = (mask, mixed, padded, turned, scores, weights, stats, blend)
+    one = Attention(query_one, kv_one, table_one, *shared)
+    two = Attention(query_two, kv_two, table_two, *shared)
+    newest_first = range(segments - 1, -1, -1)
+
+    for name in ("key", "value", "docs", "query"):
         loads[name].wait()
+    for row in range(SPAN, SPAN + tok_rows, SEG):
+        one.turn_values(row)
+    for segment in newest_first:
+        one.pad_queries(segment)
+    for block in range(0, tok_rows, SEG):
+        put_column(docs[:, block : block + SEG], SPAN + block)
+    for segment in range(segments):
+        put_mask(segment, *one.bounds(segment, True))
 
     pl.semaphore_wait(barrier, expected)
 
@@ -347,43 +388,11 @@
     for distance, copies in docs_copies + first_copies:
         start_sent(distance, copies)
     loads["residual"].wait()
-    residual_copy = remote(
-        residual_full.at[my_tp], residual_full.at[my_tp], {"tp": other}
-    )
+    residual_copy = remote(residual_full.at[my_tp], residual_full.at[my_tp], {"tp": other})
     residual_copy.start()
 
-    eye = lax.broadcasted_iota(jnp.int32, (SEG, SEG), 0) == lax.broadcasted_iota(
-        jnp.int32, (SEG, SEG), 1
-    )
-
-    def put_column(numbers, place):
-        picked = jnp.where(eye, numbers.astype(jnp.float32), 0.0)
-        docs_col[place : place + SEG] = jnp.broadcast_to(
-            jnp.sum(picked, axis=1, keepdims=True), (SEG, LANES)
-        )
-
-    def put_mask(segment, low, high):
-        mine = docs[:, segment * SEG : (segment + 1) * SEG].astype(jnp.float32)
-        mine = jnp.concatenate([mine, mine], axis=1)
-        same = docs_col[low:high] == mine
-        first = segment * SEG
-        mask[segment, low - first : high - first] = jnp.where(same, 0.0, HIDDEN)
-
-    shared = (mask, mixed, padded, turned, scores, weights, stats, blend)
-    one = Attention(query_one, kv_one, table_one, *shared)
-    two = Attention(query_two, kv_two, table_two, *shared)
-    newest_first = range(segments - 1, -1, -1)
-
-    for block in range(0, tok_rows, SEG):
-        put_column(docs[:, block : block + SEG], SPAN + block)
-    for segment in range(segments):
-        put_mask(segment, *one.bounds(segment, True))
-
-    loads["query"].wait()
-    for row in range(SPAN, SPAN + tok_rows, SEG):
-        one.turn_values(row)
-    for segment in newest_first:
-        one.pad_queries(segment)
+    loads["bias_one"].wait()
+    build_bias(bias_one, table_one)
     one.run(newest_first, True)
 
     loads["bias_two"].wait()
@@ -398,72 +407,78 @@
             )
     for segment in range(segments):
         put_mask(segment, *one.bounds(segment, False))
-
-    def halo_block(layer_attention, members, waiting, done):
-        for piece, (distance, copies) in zip(pieces, waiting):
-            _, _, needed, landing = piece
-            if landing + needed > min(members) * SEG and landing not in done:
-                done.add(landing)
-                wait_arrived(distance, copies)
-                for row in range(landing, landing + needed, SEG):
-                    layer_attention.turn_values(row)
-        layer_attention.run(members, False)
-
+    residual_copy.wait_recv()
+    loads["out_one"].wait()
+
+    def halo_run(attention, waiting, after):
+        done = set()
+
+        def before(segment):
+            for (_, _, needed, landing), (distance, copies) in zip(pieces, waiting):
+                if landing + needed > segment * SEG and landing not in done:
+                    done.add(landing)
+                    wait_arrived(distance, copies)
+                    for row in range(landing, landing + needed, SEG):
+                        attention.turn_values(row)
+
+        attention.run(newest_first, False, before, after)
+
+    block_after = {min(members): (start, count) for members, start, count in blocks}
     part_copies = []
-    done = set()
-    for members, start, count in blocks:
-        halo_block(one, members, first_copies, done)
-        if start > 0:
-            loads["out_one"].wait()
+
+    def project_one(segment):
+        if segment not in block_after:
+            return
+        start, count = block_after[segment]
         rows = pl.ds(start, count)
         copies = []
         for half in range(halves):
-            part_own[half, start : start + count] = jnp.dot(
+            part = jnp.dot(
                 mixed[start : start + count],
                 w_out_one[:, half * width_local : (half + 1) * width_local],
                 preferred_element_type=jnp.float32,
             ).astype(jnp.bfloat16)
+            part_own[half, start : start + count] = part
             copy = remote(part_own.at[half, rows], part_in.at[half, rows], {"tp": other})
             copy.start()
             copies.append(copy)
+            base[half, start : start + count] = residual_full[
+                half, start : start + count
+            ].astype(jnp.float32) + part.astype(jnp.float32)
         part_copies.append(copies)
 
-    residual_copy.wait_recv()
+    halo_run(one, first_copies, project_one)
+
+    for name in ("gain", "key_w", "value_w", "query_w"):
+        loads[name].wait()
     second_copies = [None] * len(pieces)
     for (_, start, count), copies in zip(blocks, part_copies):
         rows = slice(start, start + count)
-        squares = jnp.zeros((count, 1), jnp.float32)
+        squares = jnp.zeros((count, LANES), jnp.float32)
         for half in range(halves):
             copies[half].wait_recv()
-            new = residual_full[half, rows].astype(jnp.float32) + (
-                part_own[half, rows].astype(jnp.float32) + part_in[half, rows].astype(jnp.float32)
-            )
+            new = base[half, rows] + part_in[half, rows].astype(jnp.float32)
             new = new.astype(jnp.bfloat16)
             layer[half, rows] = new
             new = new.astype(jnp.float32)
-            squares = squares + jnp.sum(new * new, axis=1, keepdims=True)
-        if start > 0:
-            loads["gain"].wait()
-        scale = lax.rsqrt(squares / (halves * width_local) + eps)
-        for half in range(halves):
             columns = slice(half * width_local, (half + 1) * width_local)
-            normed[rows, columns] = (
-                layer[half, rows].astype(jnp.float32) * scale * gain[:, columns]
-            ).astype(jnp.bfloat16)
-        if start > 0:
-            loads["key_w"].wait()
-            loads["value_w"].wait()
-        kv_two[SPAN + start : SPAN + start + count] = jnp.dot(
-            normed[rows], w_kv[...], preferred_element_type=jnp.float32
+            scaled[rows, columns] = (new * gain[:, columns]).astype(jnp.bfloat16)
+            for lane in range(0, width_local, LANES):
+                squares = squares + new[:, lane : lane + LANES] * new[:, lane : lane + LANES]
+        scale = lax.rsqrt(
+            jnp.sum(squares, axis=1, keepdims=True) / (halves * width_local) + eps
+        )
+        scales[rows] = jnp.broadcast_to(scale, (count, LANES))
+        kv_two[SPAN + start : SPAN + start + count] = (
+            jnp.dot(scaled[rows], w_kv[...], preferred_element_type=jnp.float32) * scale
         ).astype(jnp.bfloat16)
         for index, piece in enumerate(pieces):
             if start <= piece[1] < start + count:
                 second_copies[index] = (piece[0], [halo_copy(kv_two, piece)])
                 start_sent(*second_copies[index])
-    loads["query_w"].wait()
-    query_two[...] = jnp.dot(normed[...], w_query[...], preferred_element_type=jnp.float32).astype(
-        jnp.bfloat16
-    )
+    query_two[...] = (
+        jnp.dot(scaled[...], w_query[...], preferred_element_type=jnp.float32) * scales[:, 0:1]
+    ).astype(jnp.bfloat16)
     for row in range(SPAN, SPAN + tok_rows, SEG):
         two.turn_values(row)
     for segment in newest_first:
@@ -477,9 +492,11 @@
     theirs = pl.ds(pl.multiple_of(other * width_local, width_local), width_local)
     ours = pl.ds(pl.multiple_of(my_tp * width_local, width_local), width_local)
     last_copies = []
-    done = set()
-    for members, start, count in blocks:
-        halo_block(two, members, second_copies, done)
+
+    def project_two(segment):
+        if segment not in block_after:
+            return
+        start, count = block_after[segment]
         rows = pl.ds(start, count)
         part_own[0, start : start + count] = jnp.dot(
             mixed[start : start + count], w_out_two[:, theirs], preferred_element_type=jnp.float32
@@ -487,6 +504,8 @@
         copy = remote(part_own.at[0, rows], last_in.at[rows], {"tp": other})
         copy.start()
         last_copies.append(copy)
+
+    halo_run(two, second_copies, project_two)
     part_own[1] = jnp.dot(
         mixed[...], w_out_two[:, ours], preferred_element_type=jnp.float32
     ).astype(jnp.bfloat16)
@@ -562,7 +581,9 @@
             pltpu.VMEM((halves, tok_rows, width_local), bf16),
             pltpu.VMEM((tok_rows, width_local), bf16),
             pltpu.VMEM((halves, tok_rows, width_local), bf16),
+            pltpu.VMEM((halves, tok_rows, width_local), f32),
             pltpu.VMEM((tok_rows, halves * width_local), bf16),
+            pltpu.VMEM((tok_rows, LANES), f32),
             pltpu.VMEM((units, group_width, LANES), bf16),
             pltpu.VMEM((2, kv_width, pl.cdiv(SPAN + tok_rows, LANES) * LANES), bf16),
             pltpu.VMEM((units, BAND, group_width), f32),

time: 18.7 us -> 18 us (0.963)
  Pallas kernels: 17.8 us -> 17.2 us
    pallas_call x1, Pallas kernels: 17.8 us -> 17.2 us  [body(): pl.pallas_call(functools.partial(kernel, n_sp), name='two_layers', out_sh...]
where the time goes in v2:
time: 18 us; the launch traced here: 17.9 us
  Pallas kernels  17.2 us (96%)
  local copies, waits for them, and re-layouts  0.68 us (4%)
    pallas_call x1, Pallas kernels, body(): pl.pallas_call(functools.partial(kernel, n_sp), name='two_layers', out_sh...  17.2 us
    unnamed x1, local copies, waits for them, and re-layouts  0.68 us

profile of v2, /device:TPU:25, one launch (start us, length us, event | category | flops | bytes accessed | tf_op | source)
XLA Modules:
  0.0 17.9 jit_solution(13966301382634240879)
XLA Ops:
  0.0 17.2 %two_layers.1 = bf16[192,512]{1,0:T(8,128)(2,1)S(1)} custom-call(bf16[192,512]{1,0:T(8,128)(2,1)} %residual_hbm.1, bf16[192,512]{1,0:T(8,128)(2,1)} %query_hbm.1, bf16[192,128]{1,0:T(8,128)(2,1)} %key_hbm.1, bf16[192,128]{1,0:T(8,128)(2,1)} %value_hbm.1, s32[1,192]{1,0:T(1,128)} %bitcast.3, f32[8,513]{1,0:T(8,128)} %bias_one_hbm.1, ...), custom_call_target="tpu_custom_call" | custom-call | tf_op jit(solution)/shard_map/two_layers/pallas_call | solution.py:554
  17.2 0.7 %copy.15 = bf16[192,512]{1,0:T(8,128)(2,1)} copy(bf16[192,512]{1,0:T(8,128)(2,1)S(1)} %two_layers.1) | data formatting | bytes 393216

commit v3 on v2

--- a/solution.py
+++ b/solution.py
@@ -212,13 +212,8 @@
     w_query,
     w_kv,
     w_out_two,
-    bias_one,
-    bias_two,
-    gain,
-    docs,
     kv_one,
     kv_two,
-    docs_prior,
     docs_col,
     mask,
     table_one,
@@ -238,8 +233,13 @@
     turned,
     scores,
     weights,
+    blend,
+    bias_one,
+    bias_two,
+    gain,
+    docs,
+    docs_prior,
     stats,
-    blend,
     send_sem,
     recv_sem,
     load_sem,
@@ -270,10 +270,10 @@
 
     own = pl.ds(SPAN, tok_rows)
     transfers = dict(
-        bias_one=(bias_one_hbm, bias_one),
         key=(key_hbm, kv_one.at[own, pl.ds(0, kv_width)]),
         value=(value_hbm, kv_one.at[own, pl.ds(kv_width, kv_width)]),
         docs=(docs_hbm, docs),
+        bias_one=(bias_one_hbm, bias_one),
         query=(query_hbm, query_one),
         residual=(residual_hbm, residual_full.at[my_tp]),
         bias_two=(bias_two_hbm, bias_two),
@@ -361,17 +361,8 @@
     two = Attention(query_two, kv_two, table_two, *shared)
     newest_first = range(segments - 1, -1, -1)
 
-    for name in ("key", "value", "docs", "query"):
+    for name in ("key", "value", "docs"):
         loads[name].wait()
-    for row in range(SPAN, SPAN + tok_rows, SEG):
-        one.turn_values(row)
-    for segment in newest_first:
-        one.pad_queries(segment)
-    for block in range(0, tok_rows, SEG):
-        put_column(docs[:, block : block + SEG], SPAN + block)
-    for segment in range(segments):
-        put_mask(segment, *one.bounds(segment, True))
-
     pl.semaphore_wait(barrier, expected)
 
     def halo_copy(kv, piece):
@@ -391,12 +382,19 @@
     residual_copy = remote(residual_full.at[my_tp], residual_full.at[my_tp], {"tp": other})
     residual_copy.start()
 
+    loads["query"].wait()
+    for row in range(SPAN, SPAN + tok_rows, SEG):
+        one.turn_values(row)
+    for segment in newest_first:
+        one.pad_queries(segment)
+    for block in range(0, tok_rows, SEG):
+        put_column(docs[:, block : block + SEG], SPAN + block)
+    for segment in range(segments):
+        put_mask(segment, *one.bounds(segment, True))
+
     loads["bias_one"].wait()
     build_bias(bias_one, table_one)
     one.run(newest_first, True)
-
-    loads["bias_two"].wait()
-    build_bias(bias_two, table_two)
 
     for distance, copies in docs_copies:
         wait_arrived(distance, copies)
@@ -410,10 +408,10 @@
     residual_copy.wait_recv()
     loads["out_one"].wait()
 
-    def halo_run(attention, waiting, after):
-        done = set()
-
+    def halo_run(attention, waiting, members, done):
         def before(segment):
+            if segment < segments - 1:
+                segment = 0
             for (_, _, needed, landing), (distance, copies) in zip(pieces, waiting):
                 if landing + needed > segment * SEG and landing not in done:
                     done.add(landing)
@@ -421,42 +419,46 @@
                     for row in range(landing, landing + needed, SEG):
                         attention.turn_values(row)
 
-        attention.run(newest_first, False, before, after)
-
-    block_after = {min(members): (start, count) for members, start, count in blocks}
+        attention.run(members, False, before)
+
     part_copies = []
-
-    def project_one(segment):
-        if segment not in block_after:
-            return
-        start, count = block_after[segment]
+    for _, start, count in blocks:
         rows = pl.ds(start, count)
-        copies = []
-        for half in range(halves):
-            part = jnp.dot(
-                mixed[start : start + count],
+        part_copies.append(
+            [
+                remote(part_own.at[half, rows], part_in.at[half, rows], {"tp": other})
+                for half in range(halves)
+            ]
+        )
+
+    def project_one(block):
+        _, start, count = blocks[block]
+        rows = slice(start, start + count)
+        parts = [
+            jnp.dot(
+                mixed[rows],
                 w_out_one[:, half * width_local : (half + 1) * width_local],
                 preferred_element_type=jnp.float32,
             ).astype(jnp.bfloat16)
-            part_own[half, start : start + count] = part
-            copy = remote(part_own.at[half, rows], part_in.at[half, rows], {"tp": other})
+            for half in range(halves)
+        ]
+        for half, part in enumerate(parts):
+            part_own[half, rows] = part
+        for copy in part_copies[block]:
             copy.start()
-            copies.append(copy)
-            base[half, start : start + count] = residual_full[
-                half, start : start + count
-            ].astype(jnp.float32) + part.astype(jnp.float32)
-        part_copies.append(copies)
-
-    halo_run(one, first_copies, project_one)
-
-    for name in ("gain", "key_w", "value_w", "query_w"):
-        loads[name].wait()
-    second_copies = [None] * len(pieces)
-    for (_, start, count), copies in zip(blocks, part_copies):
+        for half, part in enumerate(parts):
+            base[half, rows] = residual_full[half, rows].astype(jnp.float32) + part.astype(
+                jnp.float32
+            )
+
+    second_copies = [(piece[0], [halo_copy(kv_two, piece)]) for piece in pieces]
+
+    def keys_two(block):
+        _, start, count = blocks[block]
         rows = slice(start, start + count)
         squares = jnp.zeros((count, LANES), jnp.float32)
         for half in range(halves):
-            copies[half].wait_recv()
+            part_copies[block][half].wait_recv()
             new = base[half, rows] + part_in[half, rows].astype(jnp.float32)
             new = new.astype(jnp.bfloat16)
             layer[half, rows] = new
@@ -472,13 +474,38 @@
         kv_two[SPAN + start : SPAN + start + count] = (
             jnp.dot(scaled[rows], w_kv[...], preferred_element_type=jnp.float32) * scale
         ).astype(jnp.bfloat16)
-        for index, piece in enumerate(pieces):
+        for piece, copies in zip(pieces, second_copies):
             if start <= piece[1] < start + count:
-                second_copies[index] = (piece[0], [halo_copy(kv_two, piece)])
-                start_sent(*second_copies[index])
+                start_sent(*copies)
+
+    for name in ("gain", "key_w", "value_w", "query_w"):
+        loads[name].wait()
+    done = set()
+    halo_run(one, first_copies, blocks[0][0], done)
+    project_one(0)
+
+    @pl.when(my_tp == 0)
+    def _():
+        keys_two(0)
+
+    halo_run(one, first_copies, blocks[1][0], done)
+    project_one(1)
+    loads["bias_two"].wait()
+
+    @pl.when(my_tp == 1)
+    def _():
+        build_bias(bias_two, table_two)
+        keys_two(0)
+
+    keys_two(1)
     query_two[...] = (
         jnp.dot(scaled[...], w_query[...], preferred_element_type=jnp.float32) * scales[:, 0:1]
     ).astype(jnp.bfloat16)
+
+    @pl.when(my_tp == 0)
+    def _():
+        build_bias(bias_two, table_two)
+
     for row in range(SPAN, SPAN + tok_rows, SEG):
         two.turn_values(row)
     for segment in newest_first:
@@ -491,29 +518,27 @@
     loads["out_two"].wait()
     theirs = pl.ds(pl.multiple_of(other * width_local, width_local), width_local)
     ours = pl.ds(pl.multiple_of(my_tp * width_local, width_local), width_local)
+    halo_run(two, second_copies, newest_first, set())
+    part_own[0] = jnp.dot(
+        mixed[...], w_out_two[:, theirs], preferred_element_type=jnp.float32
+    ).astype(jnp.bfloat16)
+    quarter = width_local // 2
     last_copies = []
-
-    def project_two(segment):
-        if segment not in block_after:
-            return
-        start, count = block_after[segment]
-        rows = pl.ds(start, count)
-        part_own[0, start : start + count] = jnp.dot(
-            mixed[start : start + count], w_out_two[:, theirs], preferred_element_type=jnp.float32
-        ).astype(jnp.bfloat16)
-        copy = remote(part_own.at[0, rows], last_in.at[rows], {"tp": other})
-        copy.start()
-        last_copies.append(copy)
-
-    halo_run(two, second_copies, project_two)
+    for part in range(2):
+        place = pl.ds(part * quarter, quarter)
+        last_copies.append(remote(part_own.at[0, :, place], last_in.at[:, place], {"tp": other}))
+        last_copies[-1].start()
     part_own[1] = jnp.dot(
         mixed[...], w_out_two[:, ours], preferred_element_type=jnp.float32
     ).astype(jnp.bfloat16)
-    for (_, start, count), copy in zip(blocks, last_copies):
-        rows = slice(start, start + count)
+    branch = part_own[1].astype(jnp.float32)
+    branch = branch + layer[my_tp].astype(jnp.float32)
+    for part, copy in enumerate(last_copies):
+        columns = slice(part * quarter, (part + 1) * quarter)
         copy.wait_recv()
-        branch = part_own[1, rows].astype(jnp.float32) + last_in[rows].astype(jnp.float32)
-        result_ref[rows] = (layer[my_tp, rows].astype(jnp.float32) + branch).astype(jnp.bfloat16)
+        result_ref[:, columns] = (
+            branch[:, columns] + last_in[:, columns].astype(jnp.float32)
+        ).astype(jnp.bfloat16)
 
     residual_copy.wait_send()
     for distance, copies in docs_copies + first_copies + second_copies:
@@ -562,13 +587,8 @@
             pltpu.VMEM(query_w.shape, bf16),
             pltpu.VMEM((key_w.shape[0], 2 * kv_width), bf16),
             pltpu.VMEM(out_second.shape, bf16),
-            pltpu.VMEM(bias_first.shape, f32),
-            pltpu.VMEM(bias_second.shape, f32),
-            pltpu.VMEM((1, norm_gain.shape[0]), f32),
-            pltpu.VMEM((1, tok_rows), jnp.int32),
             pltpu.VMEM((SPAN + tok_rows, 2 * kv_width), bf16),
             pltpu.VMEM((SPAN + tok_rows, 2 * kv_width), bf16),
-            pltpu.VMEM((hops, 1, tok_rows), jnp.int32),
             pltpu.VMEM((SPAN + tok_rows, LANES), f32),
             pltpu.VMEM((tok_rows // SEG, BAND, LANES), f32),
             pltpu.VMEM((kv_local, BAND, group_width), f32),
@@ -588,8 +608,13 @@
             pltpu.VMEM((2, kv_width, pl.cdiv(SPAN + tok_rows, LANES) * LANES), bf16),
             pltpu.VMEM((units, BAND, group_width), f32),
             pltpu.VMEM((units, BAND, group_width), bf16),
+            pltpu.VMEM((units, HEAD_SIZE, group_width), f32),
+            pltpu.VMEM(bias_first.shape, f32),
+            pltpu.VMEM(bias_second.shape, f32),
+            pltpu.VMEM((1, norm_gain.shape[0]), f32),
+            pltpu.VMEM((1, tok_rows), jnp.int32),
+            pltpu.VMEM((hops, 1, tok_rows), jnp.int32),
             pltpu.VMEM((units, 2, group_width), f32),
-            pltpu.VMEM((units, HEAD_SIZE, group_width), f32),
             pltpu.SemaphoreType.DMA((n_sems,)),
             pltpu.SemaphoreType.DMA((n_sems,)),
             pltpu.SemaphoreType.DMA((13,)),

time: 18 us -> 16.8 us (0.933); the launches traced: 17.9 us -> 16.5 us
  Pallas kernels: 17.2 us -> 15.8 us
    pallas_call x1, Pallas kernels: 17.2 us -> 15.8 us  [body(): pl.pallas_call(functools.partial(kernel, n_sp), name='two_layers', out_sh...]
where the time goes in v3:
time: 16.8 us; the launch traced here: 16.5 us
  Pallas kernels  15.8 us (94%)
  local copies, waits for them, and re-layouts  0.68 us (4%)
    pallas_call x1, Pallas kernels, body(): pl.pallas_call(functools.partial(kernel, n_sp), name='two_layers', out_sh...  15.8 us
    unnamed x1, local copies, waits for them, and re-layouts  0.68 us

profile of v3, /device:TPU:25, one launch (start us, length us, event | category | flops | bytes accessed | tf_op | source)
XLA Modules:
  0.0 16.5 jit_solution(2934412559065522622)
XLA Ops:
  0.0 15.8 %two_layers.1 = bf16[192,512]{1,0:T(8,128)(2,1)S(1)} custom-call(bf16[192,512]{1,0:T(8,128)(2,1)} %residual_hbm.1, bf16[192,512]{1,0:T(8,128)(2,1)} %query_hbm.1, bf16[192,128]{1,0:T(8,128)(2,1)} %key_hbm.1, bf16[192,128]{1,0:T(8,128)(2,1)} %value_hbm.1, s32[1,192]{1,0:T(1,128)} %bitcast.3, f32[8,513]{1,0:T(8,128)} %bias_one_hbm.1, ...), custom_call_target="tpu_custom_call" | custom-call | tf_op jit(solution)/shard_map/two_layers/pallas_call | solution.py:579
  15.8 0.7 %copy.15 = bf16[192,512]{1,0:T(8,128)(2,1)} copy(bf16[192,512]{1,0:T(8,128)(2,1)S(1)} %two_layers.1) | data formatting | bytes 393216

commit v4 on v3

--- a/solution.py
+++ b/solution.py
@@ -73,6 +73,7 @@
         self.query, self.kv, self.bias, self.mask, self.mixed = query, kv, bias, mask, mixed
         self.padded, self.turned, self.scores, self.weights = padded, turned, scores, weights
         self.stats, self.blend = stats, blend
+        self.cut = SPAN
         self.groups = bias.shape[0]
         self.group_size = bias.shape[2] // SEG
         self.kv_width = self.groups * HEAD_SIZE
@@ -102,12 +103,18 @@
         if row >= SEG:
             self.turned[1, :, row - SEG : row] = block
 
-    def bounds(self, segment, local):
+    def bounds(self, segment, phase):
         first = segment * SEG
-        return (max(first, SPAN), first + BAND) if local else (first, SPAN)
-
-    def score(self, segment, group, local):
-        low, high = self.bounds(segment, local)
+        cut = max(first, self.cut)
+        return {
+            "local": (max(first, SPAN), first + BAND),
+            "halo": (first, SPAN),
+            "near": (cut, SPAN),
+            "rest": (first, cut),
+        }[phase]
+
+    def score(self, segment, group, phase):
+        low, high = self.bounds(segment, phase)
         unit = self.unit(segment, group)
         band = slice(low - segment * SEG, high - segment * SEG)
         scores = lax.dot_general(
@@ -121,29 +128,34 @@
         scores = scores * (HEAD_SIZE ** (-0.5) * LOG2E) + self.bias[group, band] + mask
         self.scores[unit, band] = scores
         largest = jnp.max(scores, axis=0, keepdims=True)
-        if local:
-            self.stats[unit, 0:1] = largest
-        else:
+        if phase != "local":
             largest = jnp.maximum(largest, self.stats[unit, 0:1])
         self.state[unit] = (largest,)
 
-    def weigh(self, segment, group, local):
-        low, high = self.bounds(segment, local)
+    def weigh(self, segment, group, phase):
+        low, high = self.bounds(segment, phase)
         unit = self.unit(segment, group)
         band = slice(low - segment * SEG, high - segment * SEG)
         (largest,) = self.state[unit]
         weight = jnp.exp2(self.scores[unit, band] - largest)
         self.weights[unit, band] = weight.astype(jnp.bfloat16)
         total = jnp.sum(weight, axis=0, keepdims=True)
-        if local:
+        fade = None
+        if phase != "local":
+            fade = jnp.exp2(self.stats[unit, 0:1] - largest)
+            total = total + self.stats[unit, 1:2] * fade
+        if self.ends(segment, phase):
+            self.state[unit] = (fade, 1.0 / total)
+        else:
+            self.stats[unit, 0:1] = largest
             self.stats[unit, 1:2] = total
-        else:
-            fade = jnp.exp2(self.stats[unit, 0:1] - largest)
-            inverse = 1.0 / (total + self.stats[unit, 1:2] * fade)
-            self.state[unit] = (fade, inverse)
-
-    def gather(self, segment, group, local):
-        low, high = self.bounds(segment, local)
+            self.state[unit] = (fade,)
+
+    def ends(self, segment, phase):
+        return phase != "local" and self.bounds(segment, phase)[0] == segment * SEG
+
+    def gather(self, segment, group, phase):
+        low, high = self.bounds(segment, phase)
         unit = self.unit(segment, group)
         band = slice(low - segment * SEG, high - segment * SEG)
         odd = low // SEG % 2
@@ -157,39 +169,52 @@
             (((1,), (0,)), ((), ())),
             preferred_element_type=jnp.float32,
         )
-        if local:
+        if phase != "local":
+            blended = blended + self.blend[unit] * self.state[unit][0]
+        if not self.ends(segment, phase):
             self.blend[unit] = blended
             return
-        fade, inverse = self.state[unit]
-        blended = (blended + self.blend[unit] * fade) * inverse
+        blended = (blended * self.state[unit][1]).astype(jnp.bfloat16)
         rows = slice(segment * SEG, (segment + 1) * SEG)
         for pair in range(self.group_size // 2):
             turned = jnp.transpose(blended[:, pair * LANES : (pair + 1) * LANES])
             both = jnp.concatenate([turned[:SEG], turned[SEG:]], axis=1)
             column = (group * self.group_size + 2 * pair) * HEAD_SIZE
-            self.mixed[rows, column : column + LANES] = both.astype(jnp.bfloat16)
-
-    def run(self, segments, local, before=None, after=None):
+            self.mixed[rows, column : column + LANES] = both
+
+    def steps(self, segments, phase, arrivals=()):
         units = [(segment, group) for segment in segments for group in range(self.groups)]
+        waits = {segment: wait for segment, wait, _ in arrivals}
+        turns = {segment: rows for segment, _, rows in arrivals}
 
         def score(unit):
-            if before is not None:
-                before(unit[0])
-            self.score(*unit, local)
+            segment, group = unit
+            if group == 0 and segment in waits:
+                waits[segment]()
+            self.score(segment, group, phase)
+            if group == self.groups - 1 and segment in turns:
+                for row in turns[segment]:
+                    self.turn_values(row)
+
+        def weigh(unit):
+            self.weigh(*unit, phase)
 
         def gather(unit):
-            self.gather(*unit, local)
-            if after is not None and unit[1] == self.groups - 1:
-                after(unit[0])
-
-        score(units[0])
+            self.gather(*unit, phase)
+
+        plan = [(score, units[0])]
         for index, unit in enumerate(units):
             if index + 1 < len(units):
-                score(units[index + 1])
+                plan.append((score, units[index + 1]))
             if index > 0:
-                gather(units[index - 1])
-            self.weigh(*unit, local)
-        gather(units[-1])
+                plan.append((gather, units[index - 1]))
+            plan.append((weigh, unit))
+        plan.append((gather, units[-1]))
+        return [functools.partial(step, unit) for step, unit in plan]
+
+    def run(self, segments, phase, arrivals=()):
+        for step in self.steps(segments, phase, arrivals):
+            step()
 
 
 def kernel(
@@ -360,6 +385,7 @@
     one = Attention(query_one, kv_one, table_one, *shared)
     two = Attention(query_two, kv_two, table_two, *shared)
     newest_first = range(segments - 1, -1, -1)
+    two.cut = pieces[0][3]
 
     for name in ("key", "value", "docs"):
         loads[name].wait()
@@ -390,11 +416,11 @@
     for block in range(0, tok_rows, SEG):
         put_column(docs[:, block : block + SEG], SPAN + block)
     for segment in range(segments):
-        put_mask(segment, *one.bounds(segment, True))
+        put_mask(segment, *one.bounds(segment, "local"))
 
     loads["bias_one"].wait()
     build_bias(bias_one, table_one)
-    one.run(newest_first, True)
+    one.run(newest_first, "local")
 
     for distance, copies in docs_copies:
         wait_arrived(distance, copies)
@@ -404,22 +430,25 @@
                 docs_prior[distance - 1, :, row + block : row + block + SEG], landing + block
             )
     for segment in range(segments):
-        put_mask(segment, *one.bounds(segment, False))
+        put_mask(segment, *one.bounds(segment, "halo"))
     residual_copy.wait_recv()
     loads["out_one"].wait()
 
-    def halo_run(attention, waiting, members, done):
-        def before(segment):
-            if segment < segments - 1:
-                segment = 0
-            for (_, _, needed, landing), (distance, copies) in zip(pieces, waiting):
-                if landing + needed > segment * SEG and landing not in done:
-                    done.add(landing)
-                    wait_arrived(distance, copies)
-                    for row in range(landing, landing + needed, SEG):
-                        attention.turn_values(row)
-
-        attention.run(members, False, before)
+    def arrival(segment, waiting, which):
+        members = list(zip(pieces, waiting))[which]
+
+        def wait():
+            for _, (distance, copies) in members:
+                wait_arrived(distance, copies)
+
+        rows = [
+            row
+            for (_, _, needed, landing), _ in members
+            for row in range(landing, landing + needed, SEG)
+        ]
+        return segment, wait, rows
+
+    newest, older = newest_first[0], newest_first[1]
 
     part_copies = []
     for _, start, count in blocks:
@@ -431,7 +460,7 @@
             ]
         )
 
-    def project_one(block):
+    def project_one(block, beside=()):
         _, start, count = blocks[block]
         rows = slice(start, start + count)
         parts = [
@@ -442,6 +471,8 @@
             ).astype(jnp.bfloat16)
             for half in range(halves)
         ]
+        for step in beside:
+            step()
         for half, part in enumerate(parts):
             part_own[half, rows] = part
         for copy in part_copies[block]:
@@ -480,15 +511,26 @@
 
     for name in ("gain", "key_w", "value_w", "query_w"):
         loads[name].wait()
-    done = set()
-    halo_run(one, first_copies, blocks[0][0], done)
-    project_one(0)
+    plan = one.steps(
+        newest_first,
+        "halo",
+        (
+            arrival(newest, first_copies, slice(0, 1)),
+            arrival(older, first_copies, slice(1, None)),
+        ),
+    )
+    tail = 2 * one.groups
+    for step in plan[:-tail]:
+        step()
+    weighs, gathers = plan[-tail::2], plan[1 - tail :: 2]
+    project_one(0, weighs)
 
     @pl.when(my_tp == 0)
     def _():
         keys_two(0)
 
-    halo_run(one, first_copies, blocks[1][0], done)
+    for step in gathers:
+        step()
     project_one(1)
     loads["bias_two"].wait()
 
@@ -510,7 +552,7 @@
         two.turn_values(row)
     for segment in newest_first:
         two.pad_queries(segment)
-    two.run(newest_first, True)
+    two.run(newest_first, "local")
     for copies in part_copies:
         for copy in copies:
             copy.wait_send()
@@ -518,7 +560,12 @@
     loads["out_two"].wait()
     theirs = pl.ds(pl.multiple_of(other * width_local, width_local), width_local)
     ours = pl.ds(pl.multiple_of(my_tp * width_local, width_local), width_local)
-    halo_run(two, second_copies, newest_first, set())
+    two.run(newest_first, "near", (arrival(newest, second_copies, slice(0, 1)),))
+    two.run(
+        [segment for segment in newest_first if segment * SEG < two.cut],
+        "rest",
+        (arrival(older, second_copies, slice(1, None)),),
+    )
     part_own[0] = jnp.dot(
         mixed[...], w_out_two[:, theirs], preferred_element_type=jnp.float32
     ).astype(jnp.bfloat16)

time: 16.8 us -> 16.2 us (0.964)
  Pallas kernels: 15.8 us -> 15.3 us
    pallas_call x1, Pallas kernels: 15.8 us -> 15.3 us  [body(): pl.pallas_call(functools.partial(kernel, n_sp), name='two_layers', out_sh...]
where the time goes in v4:
time: 16.2 us; the launch traced here: 16 us
  Pallas kernels  15.3 us (94%)
  local copies, waits for them, and re-layouts  0.68 us (4%)
    pallas_call x1, Pallas kernels, body(): pl.pallas_call(functools.partial(kernel, n_sp), name='two_layers', out_sh...  15.3 us
    unnamed x1, local copies, waits for them, and re-layouts  0.68 us

profile of v4, /device:TPU:25, one launch (start us, length us, event | category | flops | bytes accessed | tf_op | source)
XLA Modules:
  0.0 16.0 jit_solution(9891799729505424098)
XLA Ops:
  0.0 15.3 %two_layers.1 = bf16[192,512]{1,0:T(8,128)(2,1)S(1)} custom-call(bf16[192,512]{1,0:T(8,128)(2,1)} %residual_hbm.1, bf16[192,512]{1,0:T(8,128)(2,1)} %query_hbm.1, bf16[192,128]{1,0:T(8,128)(2,1)} %key_hbm.1, bf16[192,128]{1,0:T(8,128)(2,1)} %value_hbm.1, s32[1,192]{1,0:T(1,128)} %bitcast.3, f32[8,513]{1,0:T(8,128)} %bias_one_hbm.1, ...), custom_call_target="tpu_custom_call" | custom-call | tf_op jit(solution)/shard_map/two_layers/pallas_call | solution.py:626
  15.3 0.7 %copy.15 = bf16[192,512]{1,0:T(8,128)(2,1)} copy(bf16[192,512]{1,0:T(8,128)(2,1)S(1)} %two_layers.1) | data formatting | bytes 393216

commit v5 on v4

--- a/solution.py
+++ b/solution.py
@@ -488,8 +488,9 @@
         _, start, count = blocks[block]
         rows = slice(start, start + count)
         squares = jnp.zeros((count, LANES), jnp.float32)
+        for copy in part_copies[block]:
+            copy.wait_recv()
         for half in range(halves):
-            part_copies[block][half].wait_recv()
             new = base[half, rows] + part_in[half, rows].astype(jnp.float32)
             new = new.astype(jnp.bfloat16)
             layer[half, rows] = new
@@ -511,25 +512,25 @@
 
     for name in ("gain", "key_w", "value_w", "query_w"):
         loads[name].wait()
-    plan = one.steps(
-        newest_first,
+    for step in one.steps(
+        newest_first[:-1],
         "halo",
         (
             arrival(newest, first_copies, slice(0, 1)),
-            arrival(older, first_copies, slice(1, None)),
+            arrival(older, first_copies, slice(1, 2)),
         ),
+    ):
+        step()
+    project_one(0)
+    plan = one.steps(
+        newest_first[-1:], "halo", (arrival(newest_first[-1], first_copies, slice(2, None)),)
     )
-    tail = 2 * one.groups
-    for step in plan[:-tail]:
-        step()
-    weighs, gathers = plan[-tail::2], plan[1 - tail :: 2]
-    project_one(0, weighs)
 
     @pl.when(my_tp == 0)
     def _():
         keys_two(0)
 
-    for step in gathers:
+    for step in plan:
         step()
     project_one(1)
     loads["bias_two"].wait()

time: 16.2 us -> 16.1 us (level)
  no operation moved by 1% of the time
where the time goes in v5:
time: 16.1 us; the launch traced here: 15.9 us
  Pallas kernels  15.2 us (94%)
  local copies, waits for them, and re-layouts  0.68 us (4%)
    pallas_call x1, Pallas kernels, body(): pl.pallas_call(functools.partial(kernel, n_sp), name='two_layers', out_sh...  15.2 us
    unnamed x1, local copies, waits for them, and re-layouts  0.68 us

profile of v5, /device:TPU:25, one launch (start us, length us, event | category | flops | bytes accessed | tf_op | source)
XLA Modules:
  0.0 15.9 jit_solution(17654704911358533962)
XLA Ops:
  0.0 15.2 %two_layers.1 = bf16[192,512]{1,0:T(8,128)(2,1)S(1)} custom-call(bf16[192,512]{1,0:T(8,128)(2,1)} %residual_hbm.1, bf16[192,512]{1,0:T(8,128)(2,1)} %query_hbm.1, bf16[192,128]{1,0:T(8,128)(2,1)} %key_hbm.1, bf16[192,128]{1,0:T(8,128)(2,1)} %value_hbm.1, s32[1,192]{1,0:T(1,128)} %bitcast.3, f32[8,513]{1,0:T(8,128)} %bias_one_hbm.1, ...), custom_call_target="tpu_custom_call" | custom-call | tf_op jit(solution)/shard_map/two_layers/pallas_call | solution.py:627
  15.3 0.7 %copy.15 = bf16[192,512]{1,0:T(8,128)(2,1)} copy(bf16[192,512]{1,0:T(8,128)(2,1)S(1)} %two_layers.1) | data formatting | bytes 393216

commit v6 on v5

--- a/solution.py
+++ b/solution.py
@@ -249,11 +249,14 @@
     residual_full,
     part_own,
     part_in,
-    last_in,
     layer,
     base,
     scaled,
     scales,
+    mixed_in,
+    w_other,
+    last_mixed,
+    w_last,
     padded,
     turned,
     scores,
@@ -420,6 +423,13 @@
 
     loads["bias_one"].wait()
     build_bias(bias_one, table_one)
+    loads["out_one"].wait()
+    weight_copy = remote(w_out_one, w_other, {"tp": other})
+
+    @pl.when(my_tp == 0)
+    def _():
+        weight_copy.start()
+
     one.run(newest_first, "local")
 
     for distance, copies in docs_copies:
@@ -432,7 +442,6 @@
     for segment in range(segments):
         put_mask(segment, *one.bounds(segment, "halo"))
     residual_copy.wait_recv()
-    loads["out_one"].wait()
 
     def arrival(segment, waiting, which):
         members = list(zip(pieces, waiting))[which]
@@ -460,23 +469,41 @@
             ]
         )
 
-    def project_one(block, beside=()):
-        _, start, count = blocks[block]
-        rows = slice(start, start + count)
-        parts = [
+    mixed_copies = []
+    for members, _, _ in blocks:
+        mixed_copies.append([])
+        for segment in members:
+            rows = pl.ds(segment * SEG, SEG)
+            mixed_copies[-1].append(remote(mixed.at[rows], mixed_in.at[rows], {"tp": other}))
+
+    def start_mixed(block):
+        @pl.when(my_tp == 0)
+        def _():
+            for copy in mixed_copies[block]:
+                copy.start()
+
+    def project(source, weight, rows):
+        return [
             jnp.dot(
-                mixed[rows],
-                w_out_one[:, half * width_local : (half + 1) * width_local],
+                source[rows],
+                weight[:, half * width_local : (half + 1) * width_local],
                 preferred_element_type=jnp.float32,
             ).astype(jnp.bfloat16)
             for half in range(halves)
         ]
-        for step in beside:
-            step()
+
+    def project_one(block):
+        _, start, count = blocks[block]
+        rows = slice(start, start + count)
+        parts = project(mixed, w_out_one, rows)
         for half, part in enumerate(parts):
             part_own[half, rows] = part
-        for copy in part_copies[block]:
-            copy.start()
+
+        @pl.when(my_tp == 1)
+        def _():
+            for copy in part_copies[block]:
+                copy.start()
+
         for half, part in enumerate(parts):
             base[half, rows] = residual_full[half, rows].astype(jnp.float32) + part.astype(
                 jnp.float32
@@ -484,14 +511,22 @@
 
     second_copies = [(piece[0], [halo_copy(kv_two, piece)]) for piece in pieces]
 
-    def keys_two(block):
+    def keys_two(block, core):
         _, start, count = blocks[block]
         rows = slice(start, start + count)
         squares = jnp.zeros((count, LANES), jnp.float32)
-        for copy in part_copies[block]:
-            copy.wait_recv()
+        if core == 0:
+            for copy in part_copies[block]:
+                copy.wait_recv()
+            parts = [part_in[half, rows] for half in range(halves)]
+        else:
+            if block == 0:
+                weight_copy.wait_recv()
+            for copy in mixed_copies[block]:
+                copy.wait_recv()
+            parts = project(mixed_in, w_other, rows)
         for half in range(halves):
-            new = base[half, rows] + part_in[half, rows].astype(jnp.float32)
+            new = base[half, rows] + parts[half].astype(jnp.float32)
             new = new.astype(jnp.bfloat16)
             layer[half, rows] = new
             new = new.astype(jnp.float32)
@@ -521,6 +556,7 @@
         ),
     ):
         step()
+    start_mixed(0)
     project_one(0)
     plan = one.steps(
         newest_first[-1:], "halo", (arrival(newest_first[-1], first_copies, slice(2, None)),)
@@ -528,19 +564,24 @@
 
     @pl.when(my_tp == 0)
     def _():
-        keys_two(0)
+        keys_two(0, 0)
 
     for step in plan:
         step()
+    start_mixed(1)
     project_one(1)
     loads["bias_two"].wait()
 
     @pl.when(my_tp == 1)
     def _():
         build_bias(bias_two, table_two)
-        keys_two(0)
-
-    keys_two(1)
+        keys_two(0, 1)
+        keys_two(1, 1)
+
+    @pl.when(my_tp == 0)
+    def _():
+        keys_two(1, 0)
+
     query_two[...] = (
         jnp.dot(scaled[...], w_query[...], preferred_element_type=jnp.float32) * scales[:, 0:1]
     ).astype(jnp.bfloat16)
@@ -553,46 +594,58 @@
         two.turn_values(row)
     for segment in newest_first:
         two.pad_queries(segment)
-    two.run(newest_first, "local")
-    for copies in part_copies:
-        for copy in copies:
-            copy.wait_send()
-
     loads["out_two"].wait()
     theirs = pl.ds(pl.multiple_of(other * width_local, width_local), width_local)
     ours = pl.ds(pl.multiple_of(my_tp * width_local, width_local), width_local)
+    last_weight = remote(w_out_two.at[:, theirs], w_last, {"tp": other})
+    last_weight.start()
+    two.run(newest_first, "local")
+
+    @pl.when(my_tp == 1)
+    def _():
+        for copies in part_copies:
+            for copy in copies:
+                copy.wait_send()
+
+    @pl.when(my_tp == 0)
+    def _():
+        weight_copy.wait_send()
+        for copies in mixed_copies:
+            for copy in copies:
+                copy.wait_send()
+
+
+    finished = (pl.ds(two.cut, tok_rows - two.cut), pl.ds(0, two.cut))
+    mixed_last = [
+        remote(mixed.at[rows], last_mixed.at[rows], {"tp": other}) for rows in finished
+    ]
     two.run(newest_first, "near", (arrival(newest, second_copies, slice(0, 1)),))
+
+    mixed_last[0].start()
     two.run(
         [segment for segment in newest_first if segment * SEG < two.cut],
         "rest",
         (arrival(older, second_copies, slice(1, None)),),
     )
-    part_own[0] = jnp.dot(
-        mixed[...], w_out_two[:, theirs], preferred_element_type=jnp.float32
-    ).astype(jnp.bfloat16)
-    quarter = width_local // 2
-    last_copies = []
-    for part in range(2):
-        place = pl.ds(part * quarter, quarter)
-        last_copies.append(remote(part_own.at[0, :, place], last_in.at[:, place], {"tp": other}))
-        last_copies[-1].start()
-    part_own[1] = jnp.dot(
-        mixed[...], w_out_two[:, ours], preferred_element_type=jnp.float32
-    ).astype(jnp.bfloat16)
-    branch = part_own[1].astype(jnp.float32)
-    branch = branch + layer[my_tp].astype(jnp.float32)
-    for part, copy in enumerate(last_copies):
-        columns = slice(part * quarter, (part + 1) * quarter)
+    mixed_last[1].start()
+    branch = jnp.dot(mixed[...], w_out_two[:, ours], preferred_element_type=jnp.float32).astype(
+        jnp.bfloat16
+    )
+    base[0] = layer[my_tp].astype(jnp.float32) + branch.astype(jnp.float32)
+    last_weight.wait_recv()
+    for copy in mixed_last:
         copy.wait_recv()
-        result_ref[:, columns] = (
-            branch[:, columns] + last_in[:, columns].astype(jnp.float32)
-        ).astype(jnp.bfloat16)
-
+    branch = jnp.dot(last_mixed[...], w_last[...], preferred_element_type=jnp.float32).astype(
+        jnp.bfloat16
+    )
+    result_ref[...] = (base[0] + branch.astype(jnp.float32)).astype(jnp.bfloat16)
+
+    last_weight.wait_send()
+    for copy in mixed_last:
+        copy.wait_send()
     residual_copy.wait_send()
     for distance, copies in docs_copies + first_copies + second_copies:
         wait_sent(distance, copies)
-    for copy in last_copies:
-        copy.wait_send()
 
 
 def body(
@@ -619,7 +672,8 @@
     halves = out_first.shape[1] // width_local
     hops = len(hops_of(tok_rows))
     units = tok_rows // SEG * kv_local
-    n_sems = hops + 2 * len(pieces_of(tok_rows)) + 1 + 2 * halves + 2
+    n_sems = hops + 2 * len(pieces_of(tok_rows)) + 1 + 2 * halves
+    n_sems += tok_rows // SEG + 1 + 3
     vmem = pl.BlockSpec(memory_space=pltpu.VMEM)
     hbm = pl.BlockSpec(memory_space=pl.ANY)
     bf16 = jnp.bfloat16
@@ -647,11 +701,14 @@
             pltpu.VMEM((halves, tok_rows, width_local), bf16),
             pltpu.VMEM((halves, tok_rows, width_local), bf16),
             pltpu.VMEM((halves, tok_rows, width_local), bf16),
-            pltpu.VMEM((tok_rows, width_local), bf16),
             pltpu.VMEM((halves, tok_rows, width_local), bf16),
             pltpu.VMEM((halves, tok_rows, width_local), f32),
             pltpu.VMEM((tok_rows, halves * width_local), bf16),
             pltpu.VMEM((tok_rows, LANES), f32),
+            pltpu.VMEM((tok_rows, query_width), bf16),
+            pltpu.VMEM(out_first.shape, bf16),
+            pltpu.VMEM((tok_rows, query_width), bf16),
+            pltpu.VMEM((out_second.shape[0], width_local), bf16),
             pltpu.VMEM((units, group_width, LANES), bf16),
             pltpu.VMEM((2, kv_width, pl.cdiv(SPAN + tok_rows, LANES) * LANES), bf16),
             pltpu.VMEM((units, BAND, group_width), f32),

time: 16.1 us -> 15.9 us (0.988)
  no operation moved by 1% of the time
where the time goes in v6:
time: 15.9 us; the launch traced here: 15.8 us
  Pallas kernels  15.1 us (95%)
  local copies, waits for them, and re-layouts  0.68 us (4%)
    pallas_call x1, Pallas kernels, body(): pl.pallas_call(functools.partial(kernel, n_sp), name='two_layers', out_sh...  15.1 us
    unnamed x1, local copies, waits for them, and re-layouts  0.68 us

profile of v6, /device:TPU:25, one launch (start us, length us, event | category | flops | bytes accessed | tf_op | source)
XLA Modules:
  0.0 15.8 jit_solution(14921517089745814375)
XLA Ops:
  0.0 15.1 %two_layers.1 = bf16[192,512]{1,0:T(8,128)(2,1)S(1)} custom-call(bf16[192,512]{1,0:T(8,128)(2,1)} %residual_hbm.1, bf16[192,512]{1,0:T(8,128)(2,1)} %query_hbm.1, bf16[192,128]{1,0:T(8,128)(2,1)} %key_hbm.1, bf16[192,128]{1,0:T(8,128)(2,1)} %value_hbm.1, s32[1,192]{1,0:T(1,128)} %bitcast.3, f32[8,513]{1,0:T(8,128)} %bias_one_hbm.1, ...), custom_call_target="tpu_custom_call" | custom-call | tf_op jit(solution)/shard_map/two_layers/pallas_call | solution.py:681
  15.1 0.7 %copy.15 = bf16[192,512]{1,0:T(8,128)(2,1)} copy(bf16[192,512]{1,0:T(8,128)(2,1)S(1)} %two_layers.1) | data formatting | bytes 393216

commit v7 on v6

--- a/solution.py
+++ b/solution.py
@@ -430,6 +430,11 @@
     def _():
         weight_copy.start()
 
+    loads["out_two"].wait()
+    theirs = pl.ds(pl.multiple_of(other * width_local, width_local), width_local)
+    ours = pl.ds(pl.multiple_of(my_tp * width_local, width_local), width_local)
+    last_weight = remote(w_out_two.at[:, theirs], w_last, {"tp": other})
+    last_weight.start()
     one.run(newest_first, "local")
 
     for distance, copies in docs_copies:
@@ -541,8 +546,9 @@
         kv_two[SPAN + start : SPAN + start + count] = (
             jnp.dot(scaled[rows], w_kv[...], preferred_element_type=jnp.float32) * scale
         ).astype(jnp.bfloat16)
-        for piece, copies in zip(pieces, second_copies):
-            if start <= piece[1] < start + count:
+        for piece, copies in reversed(list(zip(pieces, second_copies))):
+            late = core == 1 and piece[0] != pieces[0][0]
+            if block == 1 if late else start <= piece[1] < start + count:
                 start_sent(*copies)
 
     for name in ("gain", "key_w", "value_w", "query_w"):
@@ -594,11 +600,6 @@
         two.turn_values(row)
     for segment in newest_first:
         two.pad_queries(segment)
-    loads["out_two"].wait()
-    theirs = pl.ds(pl.multiple_of(other * width_local, width_local), width_local)
-    ours = pl.ds(pl.multiple_of(my_tp * width_local, width_local), width_local)
-    last_weight = remote(w_out_two.at[:, theirs], w_last, {"tp": other})
-    last_weight.start()
     two.run(newest_first, "local")
 
     @pl.when(my_tp == 1)

time: 15.9 us -> 15.9 us (level)
  no operation moved by 1% of the time
where the time goes in v7:
time: 15.9 us; the launch traced here: 15.8 us
  Pallas kernels  15.1 us (95%)
  local copies, waits for them, and re-layouts  0.68 us (4%)
    pallas_call x1, Pallas kernels, body(): pl.pallas_call(functools.partial(kernel, n_sp), name='two_layers', out_sh...  15.1 us
    unnamed x1, local copies, waits for them, and re-layouts  0.68 us

profile of v7, /device:TPU:25, one launch (start us, length us, event | category | flops | bytes accessed | tf_op | source)
XLA Modules:
  0.0 15.8 jit_solution(7437927967969569996)
XLA Ops:
  0.0 15.1 %two_layers.1 = bf16[192,512]{1,0:T(8,128)(2,1)S(1)} custom-call(bf16[192,512]{1,0:T(8,128)(2,1)} %residual_hbm.1, bf16[192,512]{1,0:T(8,128)(2,1)} %query_hbm.1, bf16[192,128]{1,0:T(8,128)(2,1)} %key_hbm.1, bf16[192,128]{1,0:T(8,128)(2,1)} %value_hbm.1, s32[1,192]{1,0:T(1,128)} %bitcast.3, f32[8,513]{1,0:T(8,128)} %bias_one_hbm.1, ...), custom_call_target="tpu_custom_call" | custom-call | tf_op jit(solution)/shard_map/two_layers/pallas_call | solution.py:682
  15.1 0.7 %copy.15 = bf16[192,512]{1,0:T(8,128)(2,1)} copy(bf16[192,512]{1,0:T(8,128)(2,1)S(1)} %two_layers.1) | data formatting | bytes 393216

commit v8 on v7

--- a/solution.py
+++ b/solution.py
@@ -215,6 +215,19 @@
     def run(self, segments, phase, arrivals=()):
         for step in self.steps(segments, phase, arrivals):
             step()
+
+
+    def run_keys_first(self, segments, phase, values):
+        units = [(segment, group) for segment in segments for group in range(self.groups)]
+        for unit in units:
+            self.score(*unit, phase)
+        for unit in units[:2]:
+            self.weigh(*unit, phase)
+        values()
+        for index, unit in enumerate(units):
+            self.gather(*unit, phase)
+            if index + 2 < len(units):
+                self.weigh(*units[index + 2], phase)
 
 
 def kernel(
@@ -394,10 +407,13 @@
         loads[name].wait()
     pl.semaphore_wait(barrier, expected)
 
-    def halo_copy(kv, piece):
+    def halo_copy(kv, piece, column=0, width=2 * kv_width):
         distance, row, needed, landing = piece
+        columns = pl.ds(column, width)
         return remote(
-            kv.at[pl.ds(SPAN + row, needed)], kv.at[pl.ds(landing, needed)], ahead(distance)
+            kv.at[pl.ds(SPAN + row, needed), columns],
+            kv.at[pl.ds(landing, needed), columns],
+            ahead(distance),
         )
 
     docs_copies = [
@@ -514,7 +530,10 @@
                 jnp.float32
             )
 
-    second_copies = [(piece[0], [halo_copy(kv_two, piece)]) for piece in pieces]
+    second_copies = [
+        (piece[0], [halo_copy(kv_two, piece, part * kv_width, kv_width) for part in range(2)])
+        for piece in pieces
+    ]
 
     def keys_two(block, core):
         _, start, count = blocks[block]
@@ -620,14 +639,24 @@
     mixed_last = [
         remote(mixed.at[rows], last_mixed.at[rows], {"tp": other}) for rows in finished
     ]
-    two.run(newest_first, "near", (arrival(newest, second_copies, slice(0, 1)),))
-
+    def attend_two(members, phase, which):
+        landed = list(zip(pieces, second_copies))[which]
+        for _, (distance, copies) in landed:
+            wait_arrived(distance, copies[:1])
+
+        def values():
+            for _, (distance, copies) in landed:
+                wait_arrived(distance, copies[1:])
+            for (_, _, needed, landing), _ in landed:
+                for row in range(landing, landing + needed, SEG):
+                    two.turn_values(row)
+
+        two.run_keys_first(members, phase, values)
+
+    attend_two(newest_first, "near", slice(0, 1))
     mixed_last[0].start()
-    two.run(
-        [segment for segment in newest_first if segment * SEG < two.cut],
-        "rest",
-        (arrival(older, second_copies, slice(1, None)),),
-    )
+    older_two = [segment for segment in newest_first if segment * SEG < two.cut]
+    attend_two(older_two, "rest", slice(1, None))
     mixed_last[1].start()
     branch = jnp.dot(mixed[...], w_out_two[:, ours], preferred_element_type=jnp.float32).astype(
         jnp.bfloat16
@@ -673,7 +702,7 @@
     halves = out_first.shape[1] // width_local
     hops = len(hops_of(tok_rows))
     units = tok_rows // SEG * kv_local
-    n_sems = hops + 2 * len(pieces_of(tok_rows)) + 1 + 2 * halves
+    n_sems = hops + 3 * len(pieces_of(tok_rows)) + 1 + 2 * halves
     n_sems += tok_rows // SEG + 1 + 3
     vmem = pl.BlockSpec(memory_space=pltpu.VMEM)
     hbm = pl.BlockSpec(memory_space=pl.ANY)

time: 15.9 us -> 15.8 us (level)
  no operation moved by 1% of the time
where the time goes in v8:
time: 15.8 us; the launch traced here: 15.7 us
  Pallas kernels  15 us (95%)
  local copies, waits for them, and re-layouts  0.68 us (4%)
    pallas_call x1, Pallas kernels, body(): pl.pallas_call(functools.partial(kernel, n_sp), name='two_layers', out_sh...  15 us
    unnamed x1, local copies, waits for them, and re-layouts  0.68 us

profile of v8, /device:TPU:25, one launch (start us, length us, event | category | flops | bytes accessed | tf_op | source)
XLA Modules:
  0.0 15.7 jit_solution(10286256443727429708)
XLA Ops:
  0.0 15.0 %two_layers.1 = bf16[192,512]{1,0:T(8,128)(2,1)S(1)} custom-call(bf16[192,512]{1,0:T(8,128)(2,1)} %residual_hbm.1, bf16[192,512]{1,0:T(8,128)(2,1)} %query_hbm.1, bf16[192,128]{1,0:T(8,128)(2,1)} %key_hbm.1, bf16[192,128]{1,0:T(8,128)(2,1)} %value_hbm.1, s32[1,192]{1,0:T(1,128)} %bitcast.3, f32[8,513]{1,0:T(8,128)} %bias_one_hbm.1, ...), custom_call_target="tpu_custom_call" | custom-call | tf_op jit(solution)/shard_map/two_layers/pallas_call | solution.py:711
  15.0 0.7 %copy.15 = bf16[192,512]{1,0:T(8,128)(2,1)} copy(bf16[192,512]{1,0:T(8,128)(2,1)S(1)} %two_layers.1) | data formatting | bytes 393216
